TPU v7x, 512 devices: a whole 4x8x8 slice. The times are simulated.
512 devices in a mesh: sp: 128 (over z, y, core), tp: 4 (over x).
Axes of the slice: x: 4, y: 8, z: 8, core: 2. Of those that a mesh axis runs over, the one named last changes fastest.
Arguments:
- tokens: bfloat16 [16384, 2048], P(('sp', 'tp')), may hold values from -6 to 6
- norm_gain: float32 [2048], replicated, may hold values from 0.1 to 1.9
- w_query: bfloat16 [2048, 1024], P(None, 'tp'), may hold values from -3 to 3
- w_key: bfloat16 [2048, 1024], P(None, 'tp'), may hold values from -0.15625 to 0.15625
- w_value: bfloat16 [2048, 1024], P(None, 'tp'), may hold values from -0.125 to 0.125
- w_state_in: bfloat16 [2048, 512], P(None, 'tp'), may hold values from -0.125 to 0.125
- decay_rate: float32 [32, 64], P('tp'), may hold values from 0 to 0.04, as said below
- rotation: float32 [32, 64], P('tp'), may hold values from -0.5 to 0.5
- extra_decay: float32 [16384, 32], P('sp', 'tp'), may hold values from -1 to 0, as said below
- in_map: float32 [2, 32, 64, 16], P(None, 'tp'), may hold values from -1 to 1
- out_map: float32 [2, 32, 16, 64], P(None, 'tp'), may hold values from -0.5 to 0.5
- skip_gain: float32 [32, 16], P('tp'), may hold values from -4 to 4
- init_state: float32 [8, 2, 32, 64], P(None, None, 'tp'), may hold values from -6 to 6
- mix_lambda: float32 [8], P('tp'), may hold values from 0.3 to 0.8
- sub_gain: float32 [128], replicated, may hold values from 0.1 to 1.9
- w_out_state: bfloat16 [512, 2048], P('tp', 'sp'), may hold values from -0.375 to 0.375
- w_out_attn: bfloat16 [1024, 2048], P('tp', 'sp'), may hold values from -0.1875 to 0.1875
Outputs:
- mixed_out: bfloat16 [16384, 2048], P(('sp', 'tp'))
Inputs may be any that keep to these rules, and one draw needn't show every extreme that they name: `decay_rate`: positive. `extra_decay`: never positive.
All inputs are finite; a program needn't handle non-finite values.
Results may differ from a plain program's by a relative error of at most 0.017.
The roundings to bfloat16 on the way count: a program that leaves them out, or rounds other values in their place, can miss the bound.
Values may be sent and summed in bfloat16 or wider, within the bound.
No kernel may reach another device: no remote copies, remote signals or barrier semaphores. Data moves between devices by JAX's collectives and lax.ppermute only.
A program may use at most 128 MiB of HBM per device.

v0:
```python
import jax
import jax.numpy as jnp
from jax import lax
from jax.experimental import pallas as pl
from jax.experimental.pallas import tpu as pltpu
from jax.sharding import Mesh
from jax.sharding import PartitionSpec as P

SP = ("z", "h", "q", "c")
SP_TP = ("z", "h", "q", "c", "tp")

EPSILON = 1e-06
ROTARY_BASE = 10000.0
LAMBDA_INIT = 0.2
MASK_FLOOR = -1e30
ROWS = 128
SUBS = 8
STEPS = ROWS // SUBS
LANES = 128
QK_DIM = 64
SEGMENT = 64
STATE_WIDTH = 512
GROUPS = 8
GROUP = 16
STATES = 64
EL_ROWS = 16
RING = 8


f32 = jnp.float32
bf16 = jnp.bfloat16


def dot(a, b):
    return jnp.dot(a, b, preferred_element_type=f32)


def dot_nt(a, b):
    return lax.dot_general(a, b, (((1,), (1,)), ((), ())), preferred_element_type=f32)


def split_two(x):
    high = x.astype(bf16)
    return high, (x - high.astype(f32)).astype(bf16)


def row_order(transposed):
    first = lax.broadcasted_iota(jnp.int32, (ROWS, ROWS), 0)
    second = lax.broadcasted_iota(jnp.int32, (ROWS, ROWS), 1)
    row, token = (second, first) if transposed else (first, second)
    return (row % SUBS) * STEPS + row // SUBS == token


def flat_rows(x):
    twice = jnp.concatenate([x, x], axis=1)
    low = lax.broadcasted_iota(jnp.int32, (1, LANES), 1) < STATES
    tiles = [
        jnp.where(low, twice[2 * t : 2 * t + 1], twice[2 * t + 1 : 2 * t + 2])
        for t in range(GROUPS // 2)
    ]
    return jnp.concatenate(tiles, axis=1)


def wide_transitions(extra, decay, cosine, sine):
    group = lax.broadcasted_iota(jnp.int32, (GROUPS, STATE_WIDTH), 0)
    lane = lax.broadcasted_iota(jnp.int32, (GROUPS, STATE_WIDTH), 1)
    widen = (lane // STATES == group).astype(f32)
    highest = lax.Precision.HIGHEST
    ordered = jnp.dot(
        row_order(False).astype(f32), extra, precision=highest, preferred_element_type=f32
    )
    wide = jnp.dot(ordered, widen, precision=highest, preferred_element_type=f32)
    magnitude = jnp.exp(wide - flat_rows(decay))
    return magnitude * flat_rows(cosine), magnitude * flat_rows(sine)


def running_products(real, imag, store):
    run_re, run_im = real[:SUBS], imag[:SUBS]
    store(slice(0, SUBS), run_re, run_im)
    for step in range(1, STEPS):
        rows = slice(step * SUBS, (step + 1) * SUBS)
        tr, ti = real[rows], imag[rows]
        run_re, run_im = tr * run_re - ti * run_im, tr * run_im + ti * run_re
        store(rows, run_re, run_im)
    return run_re, run_im


def block_diagonal(compact, scale):
    row = lax.broadcasted_iota(jnp.int32, (GROUPS * GROUP, STATE_WIDTH), 0)
    column = lax.broadcasted_iota(jnp.int32, (GROUPS * GROUP, STATE_WIDTH), 1)
    twice = jnp.concatenate([compact, compact], axis=1)
    spread = jnp.concatenate([twice] * (STATE_WIDTH // LANES), axis=1)
    return split_two(jnp.where(row // GROUP == column // STATES, spread * scale, 0.0))


def put_pair(ref, rows, re, im):
    ref[rows, :STATE_WIDTH] = re
    ref[rows, STATE_WIDTH:] = im


def put_split(ref, maps, scales):
    for part in range(2):
        columns = slice(part * STATE_WIDTH, (part + 1) * STATE_WIDTH)
        high, low = block_diagonal(maps[part], scales[part])
        ref[0, :, columns] = high
        ref[1, :, columns] = low


ALL = slice(None)


def prelude_kernel(extra, decay, cosine, sine, in_scale, in_map, trans, last, in_split):
    real, imag = wide_transitions(extra[...], decay[...], cosine[...], sine[...])
    put_pair(trans, ALL, real, imag)
    put_pair(last, ALL, *running_products(real, imag, lambda rows, re, im: None))
    scale = flat_rows(in_scale[...])
    put_split(in_split, in_map, (scale, scale))


def fan_kernel(one, out):
    for i in range(out.shape[0]):
        out[i] = one[...]


def scan_blocks(inject, trans, last, store):
    run_re, run_im = inject[:SUBS, :STATE_WIDTH], inject[:SUBS, STATE_WIDTH:]
    store(slice(0, SUBS), run_re, run_im)
    for step in range(1, STEPS):
        rows = slice(step * SUBS, (step + 1) * SUBS)
        tr, ti = trans[rows, :STATE_WIDTH], trans[rows, STATE_WIDTH:]
        run_re, run_im = (
            tr * run_re - ti * run_im + inject[rows, :STATE_WIDTH],
            tr * run_im + ti * run_re + inject[rows, STATE_WIDTH:],
        )
        store(rows, run_re, run_im)
    last_re, last_im = last
    add = (jnp.zeros((1, STATE_WIDTH), f32), jnp.zeros((1, STATE_WIDTH), f32))
    mult = (jnp.ones((1, STATE_WIDTH), f32), jnp.zeros((1, STATE_WIDTH), f32))
    starts = []
    for sub in range(SUBS):
        starts.append((*mult, *add))
        one = slice(sub, sub + 1)
        tr, ti = last_re[one], last_im[one]
        add = (
            tr * add[0] - ti * add[1] + run_re[one],
            tr * add[1] + ti * add[0] + run_im[one],
        )
        mult = (tr * mult[0] - ti * mult[1], tr * mult[1] + ti * mult[0])
    return starts, (*mult, *add)


def inject_of(drive, in_split):
    return dot(drive, in_split[0]) + dot(drive, in_split[1])


def project_kernel(
    place,
    tokens,
    gain,
    w_query,
    w_key,
    last,
    cosine,
    sine,
    trans,
    in_split,
    w_value_far,
    w_state_far,
    keep,
    send,
    drive_out,
    w_value,
    w_state,
    arrived,
):
    copies = [
        pltpu.make_async_copy(far, near, arrived.at[i])
        for i, (far, near) in enumerate(
            (
                (w_state_far, w_state),
                (w_value_far, w_value),
            )
        )
    ]
    for copy in copies:
        copy.start()
    head = place[1]
    wide = tokens[...].astype(f32)
    scale = lax.rsqrt(jnp.mean(wide * wide, axis=-1, keepdims=True) + EPSILON)
    normed = (wide * scale * gain[...]).astype(bf16)
    copies[0].wait()
    drive = dot(normed, w_state[...]).astype(bf16)
    ordered = dot(row_order(False).astype(bf16), drive).astype(bf16)
    drive_out[...] = ordered
    inject = inject_of(ordered, in_split)
    _, element_parts = scan_blocks(
        inject,
        trans,
        (last[:, :STATE_WIDTH], last[:, STATE_WIDTH:]),
        lambda rows, re, im: None,
    )
    parts = [
        member[:, tile * LANES : (tile + 1) * LANES]
        for member in element_parts
        for tile in range(STATE_WIDTH // LANES)
    ]
    element = jnp.concatenate(parts, axis=0).astype(bf16)
    keep[3 * ROWS :, :] = element
    send[3 * ROWS :, :] = element

    lane = lax.broadcasted_iota(jnp.int32, (ROWS, LANES), 1)
    first_half = lane % QK_DIM < QK_DIM // 2
    cos, sin = cosine[...], sine[...]

    def turned(half):
        other = jnp.where(
            first_half,
            pltpu.roll(half, LANES - QK_DIM // 2, 1),
            pltpu.roll(half, QK_DIM // 2, 1),
        )
        return half * cos + other * sin

    def put(at, first, second):
        rows = slice(at * ROWS, (at + 1) * ROWS)
        keep[rows, :] = jnp.where(head == 0, first, second)
        send[rows, :] = jnp.where(head == 0, second, first)

    query = dot(normed, w_query[...])
    key = dot(normed, w_key[...])
    copies[1].wait()
    value = dot(normed, w_value[...])
    put(0, turned(key[:, :LANES]).astype(bf16), turned(key[:, LANES:]).astype(bf16))
    put(1, value[:, :LANES].astype(bf16), value[:, LANES:].astype(bf16))
    put(
        2,
        turned(query[:, :LANES]).astype(bf16) * QK_DIM**-0.5,
        turned(query[:, LANES:]).astype(bf16) * QK_DIM**-0.5,
    )


def join_kernel(keep, got, out):
    for part in range(2):
        rows = slice(part * ROWS, (part + 1) * ROWS)
        out[2 * part * ROWS : (2 * part + 1) * ROWS, :] = keep[rows, :]
        out[(2 * part + 1) * ROWS : 2 * (part + 1) * ROWS, :] = got[rows, :]
    out[4 * ROWS : 4 * ROWS + EL_ROWS, :] = keep[3 * ROWS :, :]
    out[4 * ROWS + EL_ROWS :, :] = got[3 * ROWS :, :]


def attention_kernel(place, mix, sub_gain, keep, got, *rest):
    passed = rest[: RING - 1]
    out_keep, out_send, elements, scores, peak, total, numerator = rest[RING - 1 :]
    depth, head = place[0], place[1]
    pair = 2 * ROWS
    for k in range(RING - 1):
        elements[2 * EL_ROWS * k : 2 * EL_ROWS * (k + 1), :] = passed[k][2 * pair :, :]
    query = jnp.concatenate([keep[2 * ROWS : 3 * ROWS, :], got[2 * ROWS : 3 * ROWS, :]], axis=0)
    queries = (query[:, :QK_DIM], query[:, QK_DIM:])
    row = lax.broadcasted_iota(jnp.int32, (pair, pair), 0)
    column = lax.broadcasted_iota(jnp.int32, (pair, pair), 1)

    def segment(index):
        block = jnp.where(index < ROWS, head, 1 - head)
        return block * (ROWS // SEGMENT) + index % ROWS // SEGMENT

    allowed = segment(column) <= segment(row)
    own_key = jnp.concatenate([keep[:ROWS, :], got[:ROWS, :]], axis=0)
    own_value = jnp.concatenate([keep[ROWS:pair, :], got[ROWS:pair, :]], axis=0)
    for c in range(2):
        raw = dot_nt(queries[c], own_key[:, c * QK_DIM : (c + 1) * QK_DIM])
        masked = jnp.where(allowed, raw, MASK_FLOOR)
        scores[c, 0] = masked
        peak[c] = jnp.maximum(masked[:, :LANES], masked[:, LANES:])
    for k in range(1, RING):

        @pl.when(k <= depth)
        def _():
            for c in range(2):
                keys = passed[k - 1][:pair, c * QK_DIM : (c + 1) * QK_DIM]
                raw = dot_nt(queries[c], keys)
                scores[c, k] = raw
                peak[c] = jnp.maximum(peak[c], jnp.maximum(raw[:, :LANES], raw[:, LANES:]))

    tops = [jnp.max(peak[c], axis=-1, keepdims=True) for c in range(2)]
    for c in range(2):
        weight = jnp.exp(scores[c, 0] - tops[c])
        total[c] = weight[:, :LANES] + weight[:, LANES:]
        numerator[c] = dot(weight.astype(bf16), own_value)
    for k in range(1, RING):

        @pl.when(k <= depth)
        def _():
            for c in range(2):
                weight = jnp.exp(scores[c, k] - tops[c])
                total[c] += weight[:, :LANES] + weight[:, LANES:]
                numerator[c] += dot(weight.astype(bf16), passed[k - 1][pair : 2 * pair, :])

    mapped = [numerator[c] / jnp.sum(total[c], axis=-1, keepdims=True) for c in range(2)]
    difference = mapped[0] - mix[head] * mapped[1]
    mean = jnp.mean(difference * difference, axis=-1, keepdims=True)
    out = difference * lax.rsqrt(mean + EPSILON) * sub_gain[...] * (1.0 - LAMBDA_INIT)
    out_keep[...] = out[:ROWS].astype(bf16)
    out_send[...] = out[ROWS:].astype(bf16)


def state_kernel(
    place,
    init,
    got,
    elements,
    drive,
    skip,
    extra,
    decay,
    cosine,
    sine,
    in_scale,
    in_map,
    out_map,
    out,
    trans,
    product,
    in_split,
    out_split,
    states,
):
    depth, head, sequence = place[0], place[1], place[3]
    real, imag = wide_transitions(extra[...], decay[...], cosine[...], sine[...])
    put_pair(trans, ALL, real, imag)
    last = running_products(real, imag, lambda rows, re, im: put_pair(product, rows, re, im))
    scale = flat_rows(in_scale[...])
    put_split(in_split, in_map, (scale, scale))
    put_split(out_split, out_map, (1.0, -1.0))
    run_re, run_im = flat_rows(init[sequence, 0]), flat_rows(init[sequence, 1])

    def member(ref, base, index):
        tiles = STATE_WIDTH // LANES
        rows = [ref[base + index * tiles + t : base + index * tiles + t + 1, :] for t in range(tiles)]
        return jnp.concatenate(rows, axis=1).astype(f32)

    def advance(carry, ref, base, use):
        re, im = carry
        mr, mi, ar, ai = [member(ref, base, i) for i in range(4)]
        new_re, new_im = mr * re - mi * im + ar, mr * im + mi * re + ai
        return jnp.where(use, new_re, re), jnp.where(use, new_im, im)

    carry = (run_re, run_im)
    for k in range(RING - 1, 0, -1):
        use = k <= depth
        base = 2 * EL_ROWS * (k - 1)
        mine = [member(elements, base, i) for i in range(4)]
        other = [member(elements, base + EL_ROWS, i) for i in range(4)]
        early = [jnp.where(head == 0, a, b) for a, b in zip(mine, other)]
        late = [jnp.where(head == 0, b, a) for a, b in zip(mine, other)]
        for mr, mi, ar, ai in (early, late):
            re, im = carry
            new_re, new_im = mr * re - mi * im + ar, mr * im + mi * re + ai
            carry = jnp.where(use, new_re, re), jnp.where(use, new_im, im)
    carry = advance(carry, got, 3 * ROWS, head == 1)
    in_re, in_im = carry
    starts, _ = scan_blocks(
        inject_of(drive[...], in_split),
        trans,
        last,
        lambda rows, re, im: put_pair(states, rows, re, im),
    )
    add_re = jnp.concatenate([ar + mr * in_re - mi * in_im for mr, mi, ar, ai in starts], axis=0)
    add_im = jnp.concatenate([ai + mr * in_im + mi * in_re for mr, mi, ar, ai in starts], axis=0)
    for step in range(STEPS):
        rows = slice(step * SUBS, (step + 1) * SUBS)
        mr, mi = product[rows, :STATE_WIDTH], product[rows, STATE_WIDTH:]
        states[rows, :STATE_WIDTH] += mr * add_re - mi * add_im
        states[rows, STATE_WIDTH:] += mr * add_im + mi * add_re
    high, low = split_two(states[...])
    lane = lax.broadcasted_iota(jnp.int32, (GROUP, LANES), 1)
    spread = (lane % GROUP == lax.broadcasted_iota(jnp.int32, (GROUP, LANES), 0)).astype(f32)
    tiled = jnp.dot(
        skip[...], spread, precision=lax.Precision.HIGHEST, preferred_element_type=f32
    )
    own = lax.broadcasted_iota(jnp.int32, (GROUPS, LANES), 1) // GROUP
    own = own == lax.broadcasted_iota(jnp.int32, (GROUPS, LANES), 0)
    skip_row = jnp.sum(jnp.where(own, tiled, 0.0), axis=0, keepdims=True)
    mixed = (
        dot_nt(high, out_split[0])
        + dot_nt(low, out_split[0])
        + dot_nt(high, out_split[1])
        + skip_row * drive[...].astype(f32)
    )
    result = jax.nn.gelu(mixed).astype(bf16)
    out[...] = dot(row_order(True).astype(bf16), result).astype(bf16)


def output_kernel(place, state, kept, came, own, swapped_in, out, full):
    first = place[1] == 0
    mine, other = kept[...], came[...]
    acts = jnp.concatenate(
        [state[...], jnp.where(first, mine, other), jnp.where(first, other, mine)], axis=1
    )
    low_core = place[2] == 0
    for block in range(own.shape[0]):
        here, there = own[block], swapped_in[block]
        at = block % RING * 8 + block // RING
        full[at, 0] = jnp.where(low_core, here, there)
        full[at, 1] = jnp.where(low_core, there, here)
    weights = full[...].reshape(2 * own.shape[0] * own.shape[1], own.shape[2])
    out[...] = dot_nt(acts, weights).astype(bf16)


VMEM = pl.BlockSpec(memory_space=pltpu.VMEM)
SMEM = pl.BlockSpec(memory_space=pltpu.SMEM)
FAR = pl.BlockSpec(memory_space=pltpu.HBM)


def call(body, out_shapes, smem, args, scratch=(), far=0):
    near = len(args) - far
    specs = [SMEM if i in smem else VMEM if i < near else FAR for i in range(len(args))]
    return pl.pallas_call(
        body,
        out_shape=[jax.ShapeDtypeStruct(s, d) for s, d in out_shapes],
        in_specs=specs,
        out_specs=[VMEM] * len(out_shapes),
        scratch_shapes=list(scratch),
        compiler_params=pltpu.CompilerParams(vmem_limit_bytes=20 * 1024 * 1024),
    )(*args)


def sent_to_all(x, axis):
    (copies,) = call(fan_kernel, [((lax.axis_size(axis), *x.shape), x.dtype)], (), (x,))
    return lax.all_to_all(copies, axis, split_axis=0, concat_axis=0, tiled=True)


def in_hbm(x):
    return pltpu.with_memory_space_constraint(x, pltpu.HBM)


def swapped(x, axis):
    return lax.ppermute(x, axis, [(0, 1), (1, 0)])


def local(
    tokens,
    norm_gain,
    w_query,
    w_key,
    w_value,
    w_state_in,
    decay_rate,
    rotation,
    extra_decay,
    in_map,
    out_map,
    skip_gain,
    init_state,
    mix_lambda,
    sub_gain,
    w_out_state,
    w_out_attn,
):
    depth, head, core = lax.axis_index("z"), lax.axis_index("h"), lax.axis_index("c")
    sequence = lax.axis_index("q") * 2 + core
    place = jnp.stack([depth, head, core, sequence]).astype(jnp.int32)
    gathered = sent_to_all(tokens, "tp").reshape(ROWS, tokens.shape[1])

    positions = ((depth * 2 + head) * ROWS + jnp.arange(ROWS, dtype=jnp.int32)).astype(f32)
    lane = jnp.arange(LANES, dtype=jnp.int32)
    inverse = ROTARY_BASE ** (-2.0 * (lane % (QK_DIM // 2)).astype(f32) / QK_DIM)
    angles = positions[:, None] * inverse[None, :]
    cosine_table = jnp.cos(angles)
    sine_table = jnp.where(lane % QK_DIM < QK_DIM // 2, -1.0, 1.0)[None, :] * jnp.sin(angles)
    maps = (2, GROUPS * GROUP, STATES)
    wide = ((ROWS, 2 * STATE_WIDTH), f32)
    diagonal = ((2, GROUPS * GROUP, 2 * STATE_WIDTH), bf16)
    state_params = (
        extra_decay,
        decay_rate,
        jnp.cos(rotation),
        jnp.sin(rotation),
        jnp.sqrt(-jnp.expm1(-2.0 * decay_rate)),
        jnp.swapaxes(in_map, 2, 3).reshape(maps),
    )
    trans, last, in_split = call(
        prelude_kernel, [wide, ((SUBS, 2 * STATE_WIDTH), f32), diagonal], (), state_params
    )
    weights = jnp.concatenate((w_out_state, w_out_attn), axis=0).T

    payload = ((3 * ROWS + EL_ROWS, LANES), bf16)
    keep, send, drive = call(
        project_kernel,
        [payload, payload, ((ROWS, GROUPS * GROUP), bf16)],
        (0,),
        (
            place,
            gathered,
            norm_gain.reshape(1, -1),
            w_query,
            w_key,
            last,
            cosine_table,
            sine_table,
            trans,
            in_split,
            in_hbm(w_value),
            in_hbm(w_state_in),
        ),
        [
            pltpu.VMEM(w_value.shape, bf16),
            pltpu.VMEM(w_state_in.shape, bf16),
            pltpu.SemaphoreType.DMA((2,)),
        ],
        far=2,
    )
    got = swapped(send, "h")
    weights, keep = lax.optimization_barrier((weights, keep))
    weight_rows = sent_to_all(weights, "z").reshape(-1, weights.shape[1])

    (shared,) = call(join_kernel, [((4 * ROWS + 2 * EL_ROWS, LANES), bf16)], (), (keep, got))

    def along(x, pairs):
        return lax.ppermute(x, "z", pairs)

    up = lambda by, first=0: [(i, i + by) for i in range(first, RING - by)]
    two = along(shared, up(2))
    six = along(shared, [(0, 6), (1, 7), (2, 0)])
    one = along(shared, up(1))
    seven = along(shared, [(0, 7)])
    four = along(two, up(2, 2))
    three = along(two, up(1, 2))
    five = along(six, [(6, 5), (7, 6), (0, 7)])
    passed = [one, two, three, four, five, six, seven]
    weight_blocks = sent_to_all(weight_rows, ("h", "q"))

    pair = (2, 2 * ROWS, LANES)
    out_keep, out_send, elements = call(
        attention_kernel,
        [((ROWS, LANES), bf16)] * 2 + [((2 * EL_ROWS * (RING - 1), LANES), bf16)],
        (0, 1),
        (place, mix_lambda, sub_gain.reshape(1, -1), keep, got, *passed),
        [pltpu.VMEM((2, RING, 2 * ROWS, 2 * ROWS), f32)] + [pltpu.VMEM(pair, f32)] * 3,
    )
    came = swapped(out_send, "h")

    (state_out,) = call(
        state_kernel,
        [((ROWS, GROUPS * GROUP), bf16)],
        (0,),
        (place, init_state, got, elements, drive, skip_gain, *state_params, out_map.reshape(maps)),
        [
            pltpu.VMEM(wide[0], f32),
            pltpu.VMEM(wide[0], f32),
            pltpu.VMEM(diagonal[0], bf16),
            pltpu.VMEM(diagonal[0], bf16),
            pltpu.VMEM(wide[0], f32),
        ],
    )

    weight_blocks, out_keep = lax.optimization_barrier((weight_blocks, out_keep))
    other_blocks = swapped(weight_blocks, "c")
    width = w_out_attn.shape[1]
    blocks = (-1, width, weights.shape[1])

    (partial,) = call(
        output_kernel,
        [((ROWS, RING * 2 * 8 * width), bf16)],
        (0,),
        (
            place,
            state_out,
            out_keep,
            came,
            weight_blocks.reshape(blocks),
            other_blocks.reshape(blocks),
        ),
        [pltpu.VMEM((RING * 8, 2, width, weights.shape[1]), bf16)],
    )
    parts = partial.reshape(lax.axis_size("tp"), tokens.shape[0], -1)
    shares = lax.all_to_all(parts, "tp", 0, 0, tiled=True)
    return jnp.sum(shares.astype(f32), axis=0).astype(bf16)


def solution(mesh):
    split = Mesh(
        mesh.devices.reshape(8, 2, 4, 2, mesh.shape["tp"]), ("z", "h", "q", "c", "tp")
    )

    return jax.shard_map(
        local,
        mesh=split,
        in_specs=(
            P(SP_TP, None),
            P(),
            P(None, "tp"),
            P(None, "tp"),
            P(None, "tp"),
            P(None, "tp"),
            P("tp", None),
            P("tp", None),
            P(SP, "tp"),
            P(None, "tp", None, None),
            P(None, "tp", None, None),
            P("tp", None),
            P(None, None, "tp", None),
            P("tp"),
            P(),
            P("tp", SP),
            P("tp", SP),
        ),
        out_specs=P(SP_TP, None),
        check_vma=False,
    )
```

profile of v0, /device:TPU:256, one launch (start us, length us, event | category | flops | bytes accessed | tf_op | source)
XLA Modules:
  0.0 120.6 jit_solution(6143332835188212906)
XLA Ops:
  0.0 1.0 copy-done.6
  1.9 4.3 %all-to-all-start = ((bf16[4,32,2048]{2,1,0:T(8,128)(2,1)}), bf16[4,32,2048]{2,1,0:T(8,128)(2,1)S(1)}, u32[]{:S(2)}, u32[]{:S(2)}) async-start(bf16[4,32,2048]{2,1,0:T(8,128)(2,1)} %shard_map.163), calls=%async_computation | async-start | bytes 1048576 | tf_op jit(solution)/shard_map/all_to_all | solution.py:429
  12.0 0.9 fusion
  13.0 2.7 %all-to-all-done = bf16[4,32,2048]{2,1,0:T(8,128)(2,1)S(1)} async-done(((bf16[4,32,2048]{2,1,0:T(8,128)(2,1)}), bf16[4,32,2048]{2,1,0:T(8,128)(2,1)S(1)}, u32[]{:S(2)}, u32[]{:S(2)}) %all-to-all-start) | async-done | bytes 524320 | tf_op jit(solution)/shard_map/all_to_all | solution.py:429
  15.7 1.0 copy-done.4
  18.3 3.1 %shard_map.165 = (bf16[400,128]{1,0:T(8,128)(2,1)S(1)}, bf16[400,128]{1,0:T(8,128)(2,1)S(1)}, bf16[128,128]{1,0:T(8,128)(2,1)S(1)}) custom-call(s32[4]{0:T(128)S(1)} %pad_add_fusion.place, bf16[128,2048]{1,0:T(8,128)(2,1)S(1)} %bitcast.19, f32[1,2048]{1,0:T(1,128)S(1)} %bitcast.25, bf16[2048,256]{1,0:T(8,128)(2,1)S(1)} %copy-done, ...), custom_call_target="tpu_custom_call" | custom-call | tf_op jit(solution)/shard_map/pallas_call | solution.py:417
  22.0 10.3 %all_to_all.20 = bf16[8,16,384]{2,1,0:T(8,128)(2,1)S(1)} all-to-all(bf16[8,16,384]{2,1,0:T(8,128)(2,1)S(1)} %shard_map.169), channel_id=1, replica_groups=mesh['z'=8,'h'=2,'q'=4,'c'=2,'tp'=4] {'z'}, dimensions={0} | all-to-all | bytes 196608 | tf_op jit(solution)/shard_map/all_to_all | solution.py:429
  32.3 1.0 shard_map.170
  33.3 7.2 %all-to-all-start.2 = ((bf16[8,128,384]{2,1,0:T(8,128)(2,1)}), bf16[8,128,384]{2,1,0:T(8,128)(2,1)S(1)}, u32[]{:S(2)}, u32[]{:S(2)}) async-start(bf16[8,128,384]{2,1,0:T(8,128)(2,1)} %shard_map.170), calls=%async_computation.2 | async-start | bytes 1572864 | tf_op jit(solution)/shard_map/all_to_all | solution.py:429
  40.5 7.8 %collective-permute-start = (bf16[400,128]{1,0:T(8,128)(2,1)S(1)}, bf16[400,128]{1,0:T(8,128)(2,1)S(1)}, u32[]{:S(2)}, u32[]{:S(2)}) collective-permute-start(bf16[400,128]{1,0:T(8,128)(2,1)S(1)} %copy-done.20), channel_id=1, source_target_pairs={{0,32},{32,0},{1,33},{33,1},{2,34},{34,2},{3,35},{35,3},{4,36},{36... | collective-permute-start | bytes 307208 | tf_op jit(solution)/shard_map/ppermute | solution.py:437
  48.4 16.9 %collective-permute-done.got = bf16[400,128]{1,0:T(8,128)(2,1)S(1)} collective-permute-done((bf16[400,128]{1,0:T(8,128)(2,1)S(1)}, bf16[400,128]{1,0:T(8,128)(2,1)S(1)}, u32[]{:S(2)}, u32[]{:S(2)}) %collective-permute-start) | collective-permute-done | bytes 102432 | tf_op jit(solution)/shard_map/ppermute | solution.py:437
  66.0 4.8 %collective-permute-start.2 = (bf16[544,128]{1,0:T(8,128)(2,1)S(1)}, bf16[544,128]{1,0:T(8,128)(2,1)S(1)}, u32[]{:S(2)}, u32[]{:S(2)}) collective-permute-start(bf16[544,128]{1,0:T(8,128)(2,1)S(1)} %shard_map.166), channel_id=1, source_target_pairs={{0,128},{64,192},{128,256},{192,320},{256,384},{320,448},{1,129},{... | collective-permute-start | bytes 417800 | tf_op jit(solution)/shard_map/ppermute | solution.py:519
  71.4 3.0 %collective-permute-start.1 = (bf16[544,128]{1,0:T(8,128)(2,1)S(1)}, bf16[544,128]{1,0:T(8,128)(2,1)S(1)}, u32[]{:S(2)}, u32[]{:S(2)}) collective-permute-start(bf16[544,128]{1,0:T(8,128)(2,1)S(1)} %shard_map.166), channel_id=1, source_target_pairs={{0,64},{64,128},{128,192},{192,256},{256,320},{320,384},{384,448},... | collective-permute-start | bytes 417800 | tf_op jit(solution)/shard_map/ppermute | solution.py:519
  75.1 3.9 %collective-permute-done.2.rest_1_ = bf16[544,128]{1,0:T(8,128)(2,1)S(1)} collective-permute-done((bf16[544,128]{1,0:T(8,128)(2,1)S(1)}, bf16[544,128]{1,0:T(8,128)(2,1)S(1)}, u32[]{:S(2)}, u32[]{:S(2)}) %collective-permute-start.2) | collective-permute-done | bytes 139296 | tf_op jit(solution)/shard_map/ppermute | solution.py:519
  79.0 4.4 %collective-permute-start.4 = (bf16[544,128]{1,0:T(8,128)(2,1)S(1)}, bf16[544,128]{1,0:T(8,128)(2,1)S(1)}, u32[]{:S(2)}, u32[]{:S(2)}) collective-permute-start(bf16[544,128]{1,0:T(8,128)(2,1)S(1)} %collective-permute-done.2.rest_1_), channel_id=1, source_target_pairs={{128,256},{192,320},{256,384},{320,448},{129,257},{193,321},{257,3... | collective-permute-start | bytes 417800 | tf_op jit(solution)/shard_map/ppermute | solution.py:519
  83.4 3.9 %collective-permute-start.3 = (bf16[544,128]{1,0:T(8,128)(2,1)S(1)}, bf16[544,128]{1,0:T(8,128)(2,1)S(1)}, u32[]{:S(2)}, u32[]{:S(2)}) collective-permute-start(bf16[544,128]{1,0:T(8,128)(2,1)S(1)} %collective-permute-done.2.rest_1_), channel_id=1, source_target_pairs={{128,192},{192,256},{256,320},{320,384},{384,448},{129,193},{193,2... | collective-permute-start | bytes 417800 | tf_op jit(solution)/shard_map/ppermute | solution.py:519
  88.1 3.5 %collective-permute-done.3.rest_2_ = bf16[544,128]{1,0:T(8,128)(2,1)S(1)} collective-permute-done((bf16[544,128]{1,0:T(8,128)(2,1)S(1)}, bf16[544,128]{1,0:T(8,128)(2,1)S(1)}, u32[]{:S(2)}, u32[]{:S(2)}) %collective-permute-start.3) | collective-permute-done | bytes 139296 | tf_op jit(solution)/shard_map/ppermute | solution.py:519
  91.6 3.4 %shard_map.167 = (bf16[128,128]{1,0:T(8,128)(2,1)S(1)}, bf16[128,128]{1,0:T(8,128)(2,1)S(1)}, bf16[224,128]{1,0:T(8,128)(2,1)S(1)}) custom-call(s32[4]{0:T(128)S(1)} %pad_add_fusion.place, f32[2]{0:T(128)S(1)} %copy-done.17, f32[1,128]{1,0:T(1,128)S(1)} %bitcast.26, bf16[400,128]{1,0:T(8,128)(2,1)S(1)} %get-tuple-element.23.keep, ...), custom_call_target="tpu_custom_call" | custom-call | tf_op jit(solution)/shard_map/pallas_call | solution.py:417
  95.1 1.9 %collective-permute-start.9 = (bf16[8,128,384]{2,1,0:T(8,128)(2,1)S(1)}, bf16[8,128,384]{2,1,0:T(8,128)(2,1)S(1)}, u32[]{:S(2)}, u32[]{:S(2)}) collective-permute-start(bf16[8,128,384]{2,1,0:T(8,128)(2,1)S(1)} %all-to-all-done.2), channel_id=1, source_target_pairs={{0,4},{4,0},{1,5},{5,1},{2,6},{6,2},{3,7},{7,3},{8,12},{12,8},{9,1... | collective-permute-start | bytes 2359304 | tf_op jit(solution)/shard_map/ppermute | solution.py:437
  97.0 1.9 %collective-permute-start.8 = (bf16[128,128]{1,0:T(8,128)(2,1)S(1)}, bf16[128,128]{1,0:T(8,128)(2,1)S(1)}, u32[]{:S(2)}, u32[]{:S(2)}) collective-permute-start(bf16[128,128]{1,0:T(8,128)(2,1)S(1)} %get-tuple-element.29), channel_id=1, source_target_pairs={{0,32},{32,0},{1,33},{33,1},{2,34},{34,2},{3,35},{35,3},{4,36},{36... | collective-permute-start | bytes 98312 | tf_op jit(solution)/shard_map/ppermute | solution.py:437
  99.0 2.3 %shard_map.168.state = bf16[128,128]{1,0:T(8,128)(2,1)S(1)} custom-call(s32[4]{0:T(128)S(1)} %pad_add_fusion.place, f32[8,2,8,64]{3,2,1,0:T(8,128)S(1)} %copy-done.8, bf16[400,128]{1,0:T(8,128)(2,1)S(1)} %collective-permute-done.got, bf16[224,128]{1,0:T(8,128)(2,1)S(1)} %get-tuple-element.24.elements, bf16[128,128]{1,0:T(8,128)(2,1)S(1)} %copy-done.14, ...), custom_call_target="tpu_custom_call" | custom-call | tf_op jit(solution)/shard_map/pallas_call | solution.py:417
  101.3 5.5 %collective-permute-done.8.came = bf16[128,128]{1,0:T(8,128)(2,1)S(1)} collective-permute-done((bf16[128,128]{1,0:T(8,128)(2,1)S(1)}, bf16[128,128]{1,0:T(8,128)(2,1)S(1)}, u32[]{:S(2)}, u32[]{:S(2)}) %collective-permute-start.8) | collective-permute-done | bytes 32800 | tf_op jit(solution)/shard_map/ppermute | solution.py:437
  106.7 1.2 %shard_map.171 = bf16[128,2048]{1,0:T(8,128)(2,1)S(1)} custom-call(s32[4]{0:T(128)S(1)} %pad_add_fusion.place, bf16[128,128]{1,0:T(8,128)(2,1)S(1)} %shard_map.168.state, bf16[128,128]{1,0:T(8,128)(2,1)S(1)} %get-tuple-element.28.kept, bf16[128,128]{1,0:T(8,128)(2,1)S(1)} %collective-permute-done.8.came, bf16[64,16,384]{2,1,0:T(8,128)(2,1)S(1)} %bitcast.17, ...), custom_call_target="tpu_custom_call" | custom-call | tf_op jit(solution)/shard_map/pallas_call | solution.py:417
  108.0 12.0 %all_to_all.21 = bf16[4,32,2048]{2,1,0:T(8,128)(2,1)S(1)} all-to-all(bf16[4,32,2048]{2,1,0:T(8,128)(2,1)S(1)} %bitcast.18), channel_id=1, replica_groups=mesh['z'=8,'h'=2,'q'=4,'c'=2,'tp'=4] {'tp'}, dimensions={0} | all-to-all | bytes 1048576 | tf_op jit(solution)/shard_map/all_to_all | solution.py:576
  (62 shorter events, 12.3 us)
Async XLA Ops:
  0.0 8.5 %copy-start.2 = (f32[2,8,64,16]{2,3,1,0:T(8,128)S(1)}, f32[2,8,64,16]{2,3,1,0:T(8,128)}, u32[]{:S(2)}) copy-start(f32[2,8,64,16]{2,3,1,0:T(8,128)} %param.26) | copy-start | bytes 196612
  0.0 15.7 %copy-start.1 = (bf16[2048,256]{1,0:T(8,128)(2,1)S(1)}, bf16[2048,256]{1,0:T(8,128)(2,1)}, u32[]{:S(2)}) copy-start(bf16[2048,256]{1,0:T(8,128)(2,1)} %w_key.1) | copy-start | bytes 3145732
  0.0 15.7 %copy-start = (bf16[2048,256]{1,0:T(8,128)(2,1)S(1)}, bf16[2048,256]{1,0:T(8,128)(2,1)}, u32[]{:S(2)}) copy-start(bf16[2048,256]{1,0:T(8,128)(2,1)} %w_query.1) | copy-start | bytes 3145732
  1.9 13.8 %all-to-all-start = ((bf16[4,32,2048]{2,1,0:T(8,128)(2,1)}), bf16[4,32,2048]{2,1,0:T(8,128)(2,1)S(1)}, u32[]{:S(2)}, u32[]{:S(2)}) async-start(bf16[4,32,2048]{2,1,0:T(8,128)(2,1)} %shard_map.163), calls=%async_computation | async-start | bytes 1048576 | tf_op jit(solution)/shard_map/all_to_all | solution.py:429
  21.4 10.9 %copy-start.19 = (bf16[400,128]{1,0:T(8,128)(2,1)}, bf16[400,128]{1,0:T(8,128)(2,1)S(1)}, u32[]{:S(2)}) copy-start(bf16[400,128]{1,0:T(8,128)(2,1)S(1)} %get-tuple-element.21) | copy-start | bytes 307204
  33.3 7.2 %copy-start.20 = (bf16[400,128]{1,0:T(8,128)(2,1)S(1)}, bf16[400,128]{1,0:T(8,128)(2,1)}, u32[]{:S(2)}) copy-start(bf16[400,128]{1,0:T(8,128)(2,1)} %copy-done.19) | copy-start | bytes 307204
  33.3 61.8 %all-to-all-start.2 = ((bf16[8,128,384]{2,1,0:T(8,128)(2,1)}), bf16[8,128,384]{2,1,0:T(8,128)(2,1)S(1)}, u32[]{:S(2)}, u32[]{:S(2)}) async-start(bf16[8,128,384]{2,1,0:T(8,128)(2,1)} %shard_map.170), calls=%async_computation.2 | async-start | bytes 1572864 | tf_op jit(solution)/shard_map/all_to_all | solution.py:429
  40.5 24.8 %collective-permute-start = (bf16[400,128]{1,0:T(8,128)(2,1)S(1)}, bf16[400,128]{1,0:T(8,128)(2,1)S(1)}, u32[]{:S(2)}, u32[]{:S(2)}) collective-permute-start(bf16[400,128]{1,0:T(8,128)(2,1)S(1)} %copy-done.20), channel_id=1, source_target_pairs={{0,32},{32,0},{1,33},{33,1},{2,34},{34,2},{3,35},{35,3},{4,36},{36... | collective-permute-start | bytes 307208 | tf_op jit(solution)/shard_map/ppermute | solution.py:437
  65.3 26.3 %copy-start.17 = (f32[2]{0:T(128)S(1)}, f32[2]{0:T(128)}, u32[]{:S(2)}) copy-start(f32[2]{0:T(128)} %mix.1) | copy-start | bytes 28
  65.3 26.3 %copy-start.18 = (f32[128]{0:T(128)S(1)}, f32[128]{0:T(128)}, u32[]{:S(2)}) copy-start(f32[128]{0:T(128)} %param.31) | copy-start | bytes 1540
  65.3 9.1 %collective-permute-start.5 = (bf16[544,128]{1,0:T(8,128)(2,1)S(1)}, bf16[544,128]{1,0:T(8,128)(2,1)S(1)}, u32[]{:S(2)}, u32[]{:S(2)}) collective-permute-start(bf16[544,128]{1,0:T(8,128)(2,1)S(1)} %shard_map.166), channel_id=1, source_target_pairs={{0,384},{64,448},{128,0},{1,385},{65,449},{129,1},{2,386},{66,450}... | collective-permute-start | bytes 417800 | tf_op jit(solution)/shard_map/ppermute | solution.py:519
  66.0 13.0 %collective-permute-start.2 = (bf16[544,128]{1,0:T(8,128)(2,1)S(1)}, bf16[544,128]{1,0:T(8,128)(2,1)S(1)}, u32[]{:S(2)}, u32[]{:S(2)}) collective-permute-start(bf16[544,128]{1,0:T(8,128)(2,1)S(1)} %shard_map.166), channel_id=1, source_target_pairs={{0,128},{64,192},{128,256},{192,320},{256,384},{320,448},{1,129},{... | collective-permute-start | bytes 417800 | tf_op jit(solution)/shard_map/ppermute | solution.py:519
  70.8 16.6 %collective-permute-start.7 = (bf16[544,128]{1,0:T(8,128)(2,1)S(1)}, bf16[544,128]{1,0:T(8,128)(2,1)S(1)}, u32[]{:S(2)}, u32[]{:S(2)}) collective-permute-start(bf16[544,128]{1,0:T(8,128)(2,1)S(1)} %shard_map.166), channel_id=1, source_target_pairs={{0,448},{1,449},{2,450},{3,451},{4,452},{5,453},{6,454},{7,455},{8... | collective-permute-start | bytes 417800 | tf_op jit(solution)/shard_map/ppermute | solution.py:519
  71.4 15.9 %collective-permute-start.1 = (bf16[544,128]{1,0:T(8,128)(2,1)S(1)}, bf16[544,128]{1,0:T(8,128)(2,1)S(1)}, u32[]{:S(2)}, u32[]{:S(2)}) collective-permute-start(bf16[544,128]{1,0:T(8,128)(2,1)S(1)} %shard_map.166), channel_id=1, source_target_pairs={{0,64},{64,128},{128,192},{192,256},{256,320},{320,384},{384,448},... | collective-permute-start | bytes 417800 | tf_op jit(solution)/shard_map/ppermute | solution.py:519
  74.4 13.0 %collective-permute-start.6 = (bf16[544,128]{1,0:T(8,128)(2,1)S(1)}, bf16[544,128]{1,0:T(8,128)(2,1)S(1)}, u32[]{:S(2)}, u32[]{:S(2)}) collective-permute-start(bf16[544,128]{1,0:T(8,128)(2,1)S(1)} %collective-permute-done.5.rest_5_), channel_id=1, source_target_pairs={{384,320},{448,384},{0,448},{385,321},{449,385},{1,449},{386,322},... | collective-permute-start | bytes 417800 | tf_op jit(solution)/shard_map/ppermute | solution.py:519
  79.0 9.0 %collective-permute-start.4 = (bf16[544,128]{1,0:T(8,128)(2,1)S(1)}, bf16[544,128]{1,0:T(8,128)(2,1)S(1)}, u32[]{:S(2)}, u32[]{:S(2)}) collective-permute-start(bf16[544,128]{1,0:T(8,128)(2,1)S(1)} %collective-permute-done.2.rest_1_), channel_id=1, source_target_pairs={{128,256},{192,320},{256,384},{320,448},{129,257},{193,321},{257,3... | collective-permute-start | bytes 417800 | tf_op jit(solution)/shard_map/ppermute | solution.py:519
  83.4 8.2 %collective-permute-start.3 = (bf16[544,128]{1,0:T(8,128)(2,1)S(1)}, bf16[544,128]{1,0:T(8,128)(2,1)S(1)}, u32[]{:S(2)}, u32[]{:S(2)}) collective-permute-start(bf16[544,128]{1,0:T(8,128)(2,1)S(1)} %collective-permute-done.2.rest_1_), channel_id=1, source_target_pairs={{128,192},{192,256},{256,320},{320,384},{384,448},{129,193},{193,2... | collective-permute-start | bytes 417800 | tf_op jit(solution)/shard_map/ppermute | solution.py:519
  91.6 7.3 %copy-start.7 = (f32[2,8,16,64]{3,2,1,0:T(8,128)S(1)}, f32[2,8,16,64]{3,2,1,0:T(8,128)}, u32[]{:S(2)}) copy-start(f32[2,8,16,64]{3,2,1,0:T(8,128)} %param.27) | copy-start | bytes 196612
  91.6 7.4 %copy-start.8 = (f32[8,2,8,64]{3,2,1,0:T(8,128)S(1)}, f32[8,2,8,64]{3,2,1,0:T(8,128)}, u32[]{:S(2)}) copy-start(f32[8,2,8,64]{3,2,1,0:T(8,128)} %init.1) | copy-start | bytes 98308
  91.6 7.4 %copy-start.14 = (bf16[128,128]{1,0:T(8,128)(2,1)S(1)}, bf16[128,128]{1,0:T(8,128)(2,1)}, u32[]{:S(2)}) copy-start(bf16[128,128]{1,0:T(8,128)(2,1)} %copy-done.13) | copy-start | bytes 98308
  95.1 3.9 %copy-start.16 = (f32[8,16]{1,0:T(8,128)S(1)}, f32[8,16]{1,0:T(8,128)}, u32[]{:S(2)}) copy-start(f32[8,16]{1,0:T(8,128)} %skip.1) | copy-start | bytes 1540
  95.1 3.9 %copy-start.10 = (f32[8,64]{1,0:T(8,128)S(1)}, f32[8,64]{1,0:T(8,128)}, u32[]{:S(2)}) copy-start(f32[8,64]{1,0:T(8,128)} %decay.3) | copy-start | bytes 6148
  95.1 11.6 %collective-permute-start.9 = (bf16[8,128,384]{2,1,0:T(8,128)(2,1)S(1)}, bf16[8,128,384]{2,1,0:T(8,128)(2,1)S(1)}, u32[]{:S(2)}, u32[]{:S(2)}) collective-permute-start(bf16[8,128,384]{2,1,0:T(8,128)(2,1)S(1)} %all-to-all-done.2), channel_id=1, source_target_pairs={{0,4},{4,0},{1,5},{5,1},{2,6},{6,2},{3,7},{7,3},{8,12},{12,8},{9,1... | collective-permute-start | bytes 2359304 | tf_op jit(solution)/shard_map/ppermute | solution.py:437
  97.0 9.7 %collective-permute-start.8 = (bf16[128,128]{1,0:T(8,128)(2,1)S(1)}, bf16[128,128]{1,0:T(8,128)(2,1)S(1)}, u32[]{:S(2)}, u32[]{:S(2)}) collective-permute-start(bf16[128,128]{1,0:T(8,128)(2,1)S(1)} %get-tuple-element.29), channel_id=1, source_target_pairs={{0,32},{32,0},{1,33},{33,1},{2,34},{34,2},{3,35},{35,3},{4,36},{36... | collective-permute-start | bytes 98312 | tf_op jit(solution)/shard_map/ppermute | solution.py:437
  (9 other events, 9.1 us)
where the time goes:
time: 122 us; the launch traced here: 121 us
  starting transfers between devices  41.3 us (34%)
  waiting for transfers between devices  33.2 us (27%)
  blocking collectives  22.3 us (18%)
  Pallas kernels  12.5 us (10%)
  local copies, waits for them, and re-layouts  7.92 us (6%)
  other arithmetic  3.18 us (3%)
    ppermute x3, waiting for transfers between devices, swapped(): return lax.ppermute(x, axis, [(0, 1), (1, 0)])  22.4 us
    ppermute x7, starting transfers between devices, along(): return lax.ppermute(x, 'z', pairs)  18.1 us
    pallas_call x9, Pallas kernels, call(): pl.pallas_call(body, out_shape=[jax.ShapeDtypeStruct(s, d) for s, d in ou...  12.5 us
    all_to_all x1, blocking collectives, local(): shares = lax.all_to_all(parts, 'tp', 0, 0, tiled=True)  12 us
    ppermute x3, starting transfers between devices, swapped(): return lax.ppermute(x, axis, [(0, 1), (1, 0)])  11.7 us
    all_to_all x2, starting transfers between devices, sent_to_all(): return lax.all_to_all(copies, axis, split_axis=0, concat_axis=0, tiled=True)  11.5 us
    all_to_all x1, blocking collectives, sent_to_all(): return lax.all_to_all(copies, axis, split_axis=0, concat_axis=0, tiled=True)  10.3 us
    ppermute x7, waiting for transfers between devices, along(): return lax.ppermute(x, 'z', pairs)  8.12 us
  transfers between devices with their start and end apart: 12, of which 6 were waited for; matrix products, arithmetic and copies ran while one was open for 3% of the time, Pallas kernels for 5%

commit v1 on v0

--- a/solution.py
+++ b/solution.py
@@ -7,6 +7,7 @@
 from jax.sharding import PartitionSpec as P
 
 SP = ("z", "h", "q", "c")
+Y = ("h", "q")
 SP_TP = ("z", "h", "q", "c", "tp")
 
 EPSILON = 1e-06
@@ -109,10 +110,11 @@
 ALL = slice(None)
 
 
-def prelude_kernel(extra, decay, cosine, sine, in_scale, in_map, trans, last, in_split):
+def prelude_kernel(extra, decay, cosine, sine, in_scale, in_map, trans, in_split):
     real, imag = wide_transitions(extra[...], decay[...], cosine[...], sine[...])
-    put_pair(trans, ALL, real, imag)
-    put_pair(last, ALL, *running_products(real, imag, lambda rows, re, im: None))
+    put_pair(trans, slice(0, ROWS), real, imag)
+    ends = running_products(real, imag, lambda rows, re, im: None)
+    put_pair(trans, slice(ROWS, ROWS + SUBS), *ends)
     scale = flat_rows(in_scale[...])
     put_split(in_split, in_map, (scale, scale))
 
@@ -158,29 +160,29 @@
     tokens,
     gain,
     w_query,
-    w_key,
-    last,
-    cosine,
-    sine,
-    trans,
-    in_split,
+    w_key_far,
+    tables_far,
+    w_state_far,
+    split_far,
+    trans_far,
     w_value_far,
-    w_state_far,
     keep,
     send,
-    drive_out,
+    drive_far,
+    w_key,
+    tables,
+    w_state,
+    in_split,
+    trans,
     w_value,
-    w_state,
+    drive_near,
     arrived,
 ):
+    far = (w_key_far, tables_far, w_state_far, split_far, trans_far, w_value_far)
+    near = (w_key, tables, w_state, in_split, trans, w_value)
     copies = [
-        pltpu.make_async_copy(far, near, arrived.at[i])
-        for i, (far, near) in enumerate(
-            (
-                (w_state_far, w_state),
-                (w_value_far, w_value),
-            )
-        )
+        pltpu.make_async_copy(source, target, arrived.at[i])
+        for i, (source, target) in enumerate(zip(far, near))
     ]
     for copy in copies:
         copy.start()
@@ -188,29 +190,20 @@
     wide = tokens[...].astype(f32)
     scale = lax.rsqrt(jnp.mean(wide * wide, axis=-1, keepdims=True) + EPSILON)
     normed = (wide * scale * gain[...]).astype(bf16)
+
+    def put(at, first, second):
+        place_rows = slice(at * ROWS, (at + 1) * ROWS)
+        keep[place_rows, :] = jnp.where(head == 0, first, second)
+        send[place_rows, :] = jnp.where(head == 0, second, first)
+
+    query = dot(normed, w_query[...])
     copies[0].wait()
-    drive = dot(normed, w_state[...]).astype(bf16)
-    ordered = dot(row_order(False).astype(bf16), drive).astype(bf16)
-    drive_out[...] = ordered
-    inject = inject_of(ordered, in_split)
-    _, element_parts = scan_blocks(
-        inject,
-        trans,
-        (last[:, :STATE_WIDTH], last[:, STATE_WIDTH:]),
-        lambda rows, re, im: None,
-    )
-    parts = [
-        member[:, tile * LANES : (tile + 1) * LANES]
-        for member in element_parts
-        for tile in range(STATE_WIDTH // LANES)
-    ]
-    element = jnp.concatenate(parts, axis=0).astype(bf16)
-    keep[3 * ROWS :, :] = element
-    send[3 * ROWS :, :] = element
-
+    key = dot(normed, w_key[...])
+    for copy in copies[1:5]:
+        copy.wait()
     lane = lax.broadcasted_iota(jnp.int32, (ROWS, LANES), 1)
     first_half = lane % QK_DIM < QK_DIM // 2
-    cos, sin = cosine[...], sine[...]
+    cos, sin = tables[0], tables[1]
 
     def turned(half):
         other = jnp.where(
@@ -218,24 +211,38 @@
             pltpu.roll(half, LANES - QK_DIM // 2, 1),
             pltpu.roll(half, QK_DIM // 2, 1),
         )
-        return half * cos + other * sin
-
-    def put(at, first, second):
-        rows = slice(at * ROWS, (at + 1) * ROWS)
-        keep[rows, :] = jnp.where(head == 0, first, second)
-        send[rows, :] = jnp.where(head == 0, second, first)
-
-    query = dot(normed, w_query[...])
-    key = dot(normed, w_key[...])
-    copies[1].wait()
-    value = dot(normed, w_value[...])
-    put(0, turned(key[:, :LANES]).astype(bf16), turned(key[:, LANES:]).astype(bf16))
-    put(1, value[:, :LANES].astype(bf16), value[:, LANES:].astype(bf16))
+        return (half * cos + other * sin).astype(bf16)
+
+    drive = dot(normed, w_state[...]).astype(bf16)
+    ordered = dot(row_order(False).astype(bf16), drive).astype(bf16)
+    drive_near[...] = ordered
+    put(0, turned(key[:, :LANES]), turned(key[:, LANES:]))
     put(
         2,
-        turned(query[:, :LANES]).astype(bf16) * QK_DIM**-0.5,
-        turned(query[:, LANES:]).astype(bf16) * QK_DIM**-0.5,
-    )
+        turned(query[:, :LANES]) * QK_DIM**-0.5,
+        turned(query[:, LANES:]) * QK_DIM**-0.5,
+    )
+    inject = inject_of(ordered, in_split)
+    copies[5].wait()
+    leaving = pltpu.make_async_copy(drive_near, drive_far, arrived.at[6])
+    leaving.start()
+    value = dot(normed, w_value[...])
+    put(1, value[:, :LANES].astype(bf16), value[:, LANES:].astype(bf16))
+    _, element_parts = scan_blocks(
+        inject,
+        trans,
+        (trans[ROWS:, :STATE_WIDTH], trans[ROWS:, STATE_WIDTH:]),
+        lambda where, re, im: None,
+    )
+    pieces = [
+        member[:, tile * LANES : (tile + 1) * LANES]
+        for member in element_parts
+        for tile in range(STATE_WIDTH // LANES)
+    ]
+    element = jnp.concatenate(pieces, axis=0).astype(bf16)
+    keep[3 * ROWS :, :] = element
+    send[3 * ROWS :, :] = element
+    leaving.wait()
 
 
 def join_kernel(keep, got, out):
@@ -411,22 +418,23 @@
 FAR = pl.BlockSpec(memory_space=pltpu.HBM)
 
 
-def call(body, out_shapes, smem, args, scratch=(), far=0):
+def call(body, out_shapes, smem, args, scratch=(), far=0, far_out=0):
     near = len(args) - far
     specs = [SMEM if i in smem else VMEM if i < near else FAR for i in range(len(args))]
     return pl.pallas_call(
         body,
         out_shape=[jax.ShapeDtypeStruct(s, d) for s, d in out_shapes],
         in_specs=specs,
-        out_specs=[VMEM] * len(out_shapes),
+        out_specs=[VMEM] * (len(out_shapes) - far_out) + [FAR] * far_out,
         scratch_shapes=list(scratch),
         compiler_params=pltpu.CompilerParams(vmem_limit_bytes=20 * 1024 * 1024),
     )(*args)
 
 
-def sent_to_all(x, axis):
-    (copies,) = call(fan_kernel, [((lax.axis_size(axis), *x.shape), x.dtype)], (), (x,))
-    return lax.all_to_all(copies, axis, split_axis=0, concat_axis=0, tiled=True)
+def fanned(x, axis):
+    shape = (lax.axis_size(axis), *x.shape)
+    (copies,) = call(fan_kernel, [(shape, x.dtype)], (), (x,))
+    return copies
 
 
 def in_hbm(x):
@@ -459,7 +467,10 @@
     depth, head, core = lax.axis_index("z"), lax.axis_index("h"), lax.axis_index("c")
     sequence = lax.axis_index("q") * 2 + core
     place = jnp.stack([depth, head, core, sequence]).astype(jnp.int32)
-    gathered = sent_to_all(tokens, "tp").reshape(ROWS, tokens.shape[1])
+    gathered = lax.all_to_all(fanned(tokens, "tp"), "tp", 0, 0, tiled=True)
+    weights = jnp.concatenate((w_out_state, w_out_attn), axis=0).T
+    fan_weights = fanned(weights, "z")
+    gathered = gathered.reshape(ROWS, tokens.shape[1])
 
     positions = ((depth * 2 + head) * ROWS + jnp.arange(ROWS, dtype=jnp.int32)).astype(f32)
     lane = jnp.arange(LANES, dtype=jnp.int32)
@@ -478,10 +489,16 @@
         jnp.sqrt(-jnp.expm1(-2.0 * decay_rate)),
         jnp.swapaxes(in_map, 2, 3).reshape(maps),
     )
-    trans, last, in_split = call(
-        prelude_kernel, [wide, ((SUBS, 2 * STATE_WIDTH), f32), diagonal], (), state_params
-    )
-    weights = jnp.concatenate((w_out_state, w_out_attn), axis=0).T
+    tables = jnp.stack((cosine_table, sine_table))
+    trans, in_split = call(
+        prelude_kernel, [((ROWS + SUBS, 2 * STATE_WIDTH), f32), diagonal], (), state_params
+    )
+
+    fan_weights, gathered, trans, in_split, tables = lax.optimization_barrier(
+        (fan_weights, gathered, trans, in_split, tables)
+    )
+    weight_rows = lax.all_to_all(fan_weights, "z", 0, 0, tiled=True)
+    weight_rows = weight_rows.reshape(-1, weights.shape[1])
 
     payload = ((3 * ROWS + EL_ROWS, LANES), bf16)
     keep, send, drive = call(
@@ -493,26 +510,27 @@
             gathered,
             norm_gain.reshape(1, -1),
             w_query,
-            w_key,
-            last,
-            cosine_table,
-            sine_table,
-            trans,
-            in_split,
+            in_hbm(w_key),
+            in_hbm(tables),
+            in_hbm(w_state_in),
+            in_hbm(in_split),
+            in_hbm(trans),
             in_hbm(w_value),
-            in_hbm(w_state_in),
         ),
         [
+            pltpu.VMEM(w_key.shape, bf16),
+            pltpu.VMEM(tables.shape, f32),
+            pltpu.VMEM(w_state_in.shape, bf16),
+            pltpu.VMEM(in_split.shape, bf16),
+            pltpu.VMEM(trans.shape, f32),
             pltpu.VMEM(w_value.shape, bf16),
-            pltpu.VMEM(w_state_in.shape, bf16),
-            pltpu.SemaphoreType.DMA((2,)),
+            pltpu.VMEM((ROWS, GROUPS * GROUP), bf16),
+            pltpu.SemaphoreType.DMA((7,)),
         ],
-        far=2,
+        far=6,
+        far_out=1,
     )
     got = swapped(send, "h")
-    weights, keep = lax.optimization_barrier((weights, keep))
-    weight_rows = sent_to_all(weights, "z").reshape(-1, weights.shape[1])
-
     (shared,) = call(join_kernel, [((4 * ROWS + 2 * EL_ROWS, LANES), bf16)], (), (keep, got))
 
     def along(x, pairs):
@@ -527,7 +545,7 @@
     three = along(two, up(1, 2))
     five = along(six, [(6, 5), (7, 6), (0, 7)])
     passed = [one, two, three, four, five, six, seven]
-    weight_blocks = sent_to_all(weight_rows, ("h", "q"))
+    weight_blocks = lax.all_to_all(fanned(weight_rows, Y), Y, 0, 0, tiled=True)
 
     pair = (2, 2 * ROWS, LANES)
     out_keep, out_send, elements = call(
@@ -553,7 +571,6 @@
         ],
     )
 
-    weight_blocks, out_keep = lax.optimization_barrier((weight_blocks, out_keep))
     other_blocks = swapped(weight_blocks, "c")
     width = w_out_attn.shape[1]
     blocks = (-1, width, weights.shape[1])

time: 122 us -> 127 us (1.041)
  the two profiles are of different devices: /device:TPU:256 before, /device:TPU:392 now
where the time goes in v1:
time: 127 us; the launch traced here: 126 us
  blocking collectives  47 us (37%)
  waiting for transfers between devices  33.5 us (26%)
  starting transfers between devices  27.2 us (21%)
  Pallas kernels  13.4 us (11%)
  local copies, waits for them, and re-layouts  3.13 us (2%)
  other arithmetic  1.85 us (1%)
    all_to_all x1, blocking collectives, local(): weight_blocks = lax.all_to_all(fanned(weight_rows, Y), Y, 0, 0, tiled=True)  26.3 us
    ppermute x7, starting transfers between devices, along(): return lax.ppermute(x, 'z', pairs)  14.2 us
    ppermute x7, waiting for transfers between devices, along(): return lax.ppermute(x, 'z', pairs)  13.7 us
    ppermute x3, waiting for transfers between devices, swapped(): return lax.ppermute(x, axis, [(0, 1), (1, 0)])  13.7 us
    pallas_call x9, Pallas kernels, call(): pl.pallas_call(body, out_shape=[jax.ShapeDtypeStruct(s, d) for s, d in ou...  13.4 us
    all_to_all x1, blocking collectives, local(): shares = lax.all_to_all(parts, 'tp', 0, 0, tiled=True)  10.5 us
    all_to_all x1, blocking collectives, local(): weight_rows = lax.all_to_all(fan_weights, 'z', 0, 0, tiled=True)  10.2 us
    ppermute x3, starting transfers between devices, swapped(): return lax.ppermute(x, axis, [(0, 1), (1, 0)])  8.55 us
  transfers between devices with their start and end apart: 11, of which 7 were waited for; matrix products, arithmetic and copies ran while one was open for 1% of the time, Pallas kernels for 9%

profile of v1, /device:TPU:392, one launch (start us, length us, event | category | flops | bytes accessed | tf_op | source)
XLA Modules:
  0.0 126.4 jit_solution(10996746677625904508)
XLA Ops:
  0.0 0.9 copy-done.4
  1.8 4.4 %all-to-all-start = ((bf16[4,32,2048]{2,1,0:T(8,128)(2,1)}), bf16[4,32,2048]{2,1,0:T(8,128)(2,1)S(1)}, u32[]{:S(2)}, u32[]{:S(2)}) async-start(bf16[4,32,2048]{2,1,0:T(8,128)(2,1)} %shard_map.164), calls=%async_computation | async-start | bytes 1048576 | tf_op jit(solution)/shard_map/all_to_all | solution.py:470
  9.6 6.1 %all-to-all-done = bf16[4,32,2048]{2,1,0:T(8,128)(2,1)S(1)} async-done(((bf16[4,32,2048]{2,1,0:T(8,128)(2,1)}), bf16[4,32,2048]{2,1,0:T(8,128)(2,1)S(1)}, u32[]{:S(2)}, u32[]{:S(2)}) %all-to-all-start) | async-done | bytes 524320 | tf_op jit(solution)/shard_map/all_to_all | solution.py:470
  15.7 10.2 %all_to_all.20 = bf16[8,16,384]{2,1,0:T(8,128)(2,1)S(1)} all-to-all(bf16[8,16,384]{2,1,0:T(8,128)(2,1)S(1)} %shard_map.163), channel_id=1, replica_groups=mesh['z'=8,'h'=2,'q'=4,'c'=2,'tp'=4] {'z'}, dimensions={0} | all-to-all | bytes 196608 | tf_op jit(solution)/shard_map/all_to_all | solution.py:500
  25.9 26.3 %all_to_all.21 = bf16[8,128,384]{2,1,0:T(8,128)(2,1)S(1)} all-to-all(bf16[8,128,384]{2,1,0:T(8,128)(2,1)S(1)} %shard_map.170), channel_id=1, replica_groups=mesh['z'=8,'h'=2,'q'=4,'c'=2,'tp'=4] {'h','q'}, dimensions={0} | all-to-all | bytes 1572864 | tf_op jit(solution)/shard_map/all_to_all | solution.py:548
  52.3 1.9 %collective-permute-start.9 = (bf16[8,128,384]{2,1,0:T(8,128)(2,1)S(1)}, bf16[8,128,384]{2,1,0:T(8,128)(2,1)S(1)}, u32[]{:S(2)}, u32[]{:S(2)}) collective-permute-start(bf16[8,128,384]{2,1,0:T(8,128)(2,1)S(1)} %all_to_all.21), channel_id=1, source_target_pairs={{0,4},{4,0},{1,5},{5,1},{2,6},{6,2},{3,7},{7,3},{8,12},{12,8},{9,1... | collective-permute-start | bytes 2359304 | tf_op jit(solution)/shard_map/ppermute | solution.py:445
  54.9 3.8 %shard_map.166 = (bf16[400,128]{1,0:T(8,128)(2,1)S(1)}, bf16[400,128]{1,0:T(8,128)(2,1)S(1)}, bf16[128,128]{1,0:T(8,128)(2,1)S(1)}) custom-call(s32[4]{0:T(128)S(1)} %pad_add_fusion.place, bf16[128,2048]{1,0:T(8,128)(2,1)S(1)} %bitcast.19, f32[1,2048]{1,0:T(1,128)S(1)} %bitcast.25, bf16[2048,256]{1,0:T(8,128)(2,1)S(1)} %copy-done, ...), custom_call_target="tpu_custom_call" | custom-call | tf_op jit(solution)/shard_map/pallas_call | solution.py:424
  58.7 3.4 %collective-permute-start = (bf16[400,128]{1,0:T(8,128)(2,1)S(1)}, bf16[400,128]{1,0:T(8,128)(2,1)S(1)}, u32[]{:S(2)}, u32[]{:S(2)}) collective-permute-start(bf16[400,128]{1,0:T(8,128)(2,1)S(1)} %get-tuple-element.24), channel_id=1, source_target_pairs={{0,32},{32,0},{1,33},{33,1},{2,34},{34,2},{3,35},{35,3},{4,36},{36... | collective-permute-start | bytes 307208 | tf_op jit(solution)/shard_map/ppermute | solution.py:445
  62.1 9.6 %collective-permute-done.got = bf16[400,128]{1,0:T(8,128)(2,1)S(1)} collective-permute-done((bf16[400,128]{1,0:T(8,128)(2,1)S(1)}, bf16[400,128]{1,0:T(8,128)(2,1)S(1)}, u32[]{:S(2)}, u32[]{:S(2)}) %collective-permute-start) | collective-permute-done | bytes 102432 | tf_op jit(solution)/shard_map/ppermute | solution.py:445
  71.7 1.3 %collective-permute-start.5 = (bf16[544,128]{1,0:T(8,128)(2,1)S(1)}, bf16[544,128]{1,0:T(8,128)(2,1)S(1)}, u32[]{:S(2)}, u32[]{:S(2)}) collective-permute-start(bf16[544,128]{1,0:T(8,128)(2,1)S(1)} %shard_map.167), channel_id=1, source_target_pairs={{0,384},{64,448},{128,0},{1,385},{65,449},{129,1},{2,386},{66,450}... | collective-permute-start | bytes 417800 | tf_op jit(solution)/shard_map/ppermute | solution.py:537
  73.0 1.3 %collective-permute-start.2 = (bf16[544,128]{1,0:T(8,128)(2,1)S(1)}, bf16[544,128]{1,0:T(8,128)(2,1)S(1)}, u32[]{:S(2)}, u32[]{:S(2)}) collective-permute-start(bf16[544,128]{1,0:T(8,128)(2,1)S(1)} %shard_map.167), channel_id=1, source_target_pairs={{0,128},{64,192},{128,256},{192,320},{256,384},{320,448},{1,129},{... | collective-permute-start | bytes 417800 | tf_op jit(solution)/shard_map/ppermute | solution.py:537
  75.0 3.6 %collective-permute-start.1 = (bf16[544,128]{1,0:T(8,128)(2,1)S(1)}, bf16[544,128]{1,0:T(8,128)(2,1)S(1)}, u32[]{:S(2)}, u32[]{:S(2)}) collective-permute-start(bf16[544,128]{1,0:T(8,128)(2,1)S(1)} %shard_map.167), channel_id=1, source_target_pairs={{0,64},{64,128},{128,192},{192,256},{256,320},{320,384},{384,448},... | collective-permute-start | bytes 417800 | tf_op jit(solution)/shard_map/ppermute | solution.py:537
  78.6 4.3 %collective-permute-done.5.rest_5_ = bf16[544,128]{1,0:T(8,128)(2,1)S(1)} collective-permute-done((bf16[544,128]{1,0:T(8,128)(2,1)S(1)}, bf16[544,128]{1,0:T(8,128)(2,1)S(1)}, u32[]{:S(2)}, u32[]{:S(2)}) %collective-permute-start.5) | collective-permute-done | bytes 139296 | tf_op jit(solution)/shard_map/ppermute | solution.py:537
  82.8 1.9 %collective-permute-start.6 = (bf16[544,128]{1,0:T(8,128)(2,1)S(1)}, bf16[544,128]{1,0:T(8,128)(2,1)S(1)}, u32[]{:S(2)}, u32[]{:S(2)}) collective-permute-start(bf16[544,128]{1,0:T(8,128)(2,1)S(1)} %collective-permute-done.5.rest_5_), channel_id=1, source_target_pairs={{384,320},{448,384},{0,448},{385,321},{449,385},{1,449},{386,322},... | collective-permute-start | bytes 417800 | tf_op jit(solution)/shard_map/ppermute | solution.py:537
  85.2 1.3 %collective-permute-start.4 = (bf16[544,128]{1,0:T(8,128)(2,1)S(1)}, bf16[544,128]{1,0:T(8,128)(2,1)S(1)}, u32[]{:S(2)}, u32[]{:S(2)}) collective-permute-start(bf16[544,128]{1,0:T(8,128)(2,1)S(1)} %collective-permute-done.2.rest_1_), channel_id=1, source_target_pairs={{128,256},{192,320},{256,384},{320,448},{129,257},{193,321},{257,3... | collective-permute-start | bytes 417800 | tf_op jit(solution)/shard_map/ppermute | solution.py:537
  86.5 4.2 %collective-permute-start.3 = (bf16[544,128]{1,0:T(8,128)(2,1)S(1)}, bf16[544,128]{1,0:T(8,128)(2,1)S(1)}, u32[]{:S(2)}, u32[]{:S(2)}) collective-permute-start(bf16[544,128]{1,0:T(8,128)(2,1)S(1)} %collective-permute-done.2.rest_1_), channel_id=1, source_target_pairs={{128,192},{192,256},{256,320},{320,384},{384,448},{129,193},{193,2... | collective-permute-start | bytes 417800 | tf_op jit(solution)/shard_map/ppermute | solution.py:537
  90.7 4.7 %collective-permute-done.4.rest_3_ = bf16[544,128]{1,0:T(8,128)(2,1)S(1)} collective-permute-done((bf16[544,128]{1,0:T(8,128)(2,1)S(1)}, bf16[544,128]{1,0:T(8,128)(2,1)S(1)}, u32[]{:S(2)}, u32[]{:S(2)}) %collective-permute-start.4) | collective-permute-done | bytes 139296 | tf_op jit(solution)/shard_map/ppermute | solution.py:537
  95.4 4.3 %collective-permute-done.3.rest_2_ = bf16[544,128]{1,0:T(8,128)(2,1)S(1)} collective-permute-done((bf16[544,128]{1,0:T(8,128)(2,1)S(1)}, bf16[544,128]{1,0:T(8,128)(2,1)S(1)}, u32[]{:S(2)}, u32[]{:S(2)}) %collective-permute-start.3) | collective-permute-done | bytes 139296 | tf_op jit(solution)/shard_map/ppermute | solution.py:537
  99.8 4.4 %shard_map.168 = (bf16[128,128]{1,0:T(8,128)(2,1)S(1)}, bf16[128,128]{1,0:T(8,128)(2,1)S(1)}, bf16[224,128]{1,0:T(8,128)(2,1)S(1)}) custom-call(s32[4]{0:T(128)S(1)} %pad_add_fusion.place, f32[2]{0:T(128)S(1)} %copy-done.10, f32[1,128]{1,0:T(1,128)S(1)} %bitcast.26, bf16[400,128]{1,0:T(8,128)(2,1)S(1)} %get-tuple-element.25.keep, ...), custom_call_target="tpu_custom_call" | custom-call | tf_op jit(solution)/shard_map/pallas_call | solution.py:424
  104.2 3.3 %collective-permute-start.8 = (bf16[128,128]{1,0:T(8,128)(2,1)S(1)}, bf16[128,128]{1,0:T(8,128)(2,1)S(1)}, u32[]{:S(2)}, u32[]{:S(2)}) collective-permute-start(bf16[128,128]{1,0:T(8,128)(2,1)S(1)} %get-tuple-element.29), channel_id=1, source_target_pairs={{0,32},{32,0},{1,33},{33,1},{2,34},{34,2},{3,35},{35,3},{4,36},{36... | collective-permute-start | bytes 98312 | tf_op jit(solution)/shard_map/ppermute | solution.py:445
  107.5 2.3 %shard_map.169.state = bf16[128,128]{1,0:T(8,128)(2,1)S(1)} custom-call(s32[4]{0:T(128)S(1)} %pad_add_fusion.place, f32[8,2,8,64]{3,2,1,0:T(8,128)S(1)} %copy-done.6, bf16[400,128]{1,0:T(8,128)(2,1)S(1)} %collective-permute-done.got, bf16[224,128]{1,0:T(8,128)(2,1)S(1)} %get-tuple-element.26.elements, bf16[128,128]{1,0:T(8,128)(2,1)S(1)} %get-tuple-element.27.drive, ...), custom_call_target="tpu_custom_call" | custom-call | tf_op jit(solution)/shard_map/pallas_call | solution.py:424
  109.8 4.1 %collective-permute-done.8.came = bf16[128,128]{1,0:T(8,128)(2,1)S(1)} collective-permute-done((bf16[128,128]{1,0:T(8,128)(2,1)S(1)}, bf16[128,128]{1,0:T(8,128)(2,1)S(1)}, u32[]{:S(2)}, u32[]{:S(2)}) %collective-permute-start.8) | collective-permute-done | bytes 32800 | tf_op jit(solution)/shard_map/ppermute | solution.py:445
  113.9 1.2 shard_map.171
  115.2 10.5 %all_to_all.22 = bf16[4,32,2048]{2,1,0:T(8,128)(2,1)S(1)} all-to-all(bf16[4,32,2048]{2,1,0:T(8,128)(2,1)S(1)} %bitcast.18), channel_id=1, replica_groups=mesh['z'=8,'h'=2,'q'=4,'c'=2,'tp'=4] {'tp'}, dimensions={0} | all-to-all | bytes 1048576 | tf_op jit(solution)/shard_map/all_to_all | solution.py:593
  (51 shorter events, 6.8 us)
Async XLA Ops:
  0.0 0.9 copy-start.4
  1.7 4.5 %copy-start.12 = (bf16[256,16]{0,1:T(8,128)(2,1)S(1)}, bf16[256,16]{0,1:T(8,128)(2,1)}, u32[]{:S(2)}) copy-start(bf16[256,16]{0,1:T(8,128)(2,1)} %param.33) | copy-start | bytes 24580
  1.7 4.5 %copy-start.15 = (bf16[128,16]{0,1:T(8,128)(2,1)S(1)}, bf16[128,16]{0,1:T(8,128)(2,1)}, u32[]{:S(2)}) copy-start(bf16[128,16]{0,1:T(8,128)(2,1)} %param.32) | copy-start | bytes 12292
  1.7 4.5 %copy-start.7 = (f32[8,64]{1,0:T(8,128)S(1)}, f32[8,64]{1,0:T(8,128)}, u32[]{:S(2)}) copy-start(f32[8,64]{1,0:T(8,128)} %decay.3) | copy-start | bytes 6148
  1.7 4.5 %copy-start.13 = (f32[8,64]{1,0:T(8,128)S(1)}, f32[8,64]{1,0:T(8,128)}, u32[]{:S(2)}) copy-start(f32[8,64]{1,0:T(8,128)} %param.24) | copy-start | bytes 6148
  1.8 4.6 %copy-start.14 = (f32[128,8]{0,1:T(8,128)S(1)}, f32[128,8]{0,1:T(8,128)}, u32[]{:S(2)}) copy-start(f32[128,8]{0,1:T(8,128)} %param.25) | copy-start | bytes 12292
  1.8 13.9 %all-to-all-start = ((bf16[4,32,2048]{2,1,0:T(8,128)(2,1)}), bf16[4,32,2048]{2,1,0:T(8,128)(2,1)S(1)}, u32[]{:S(2)}, u32[]{:S(2)}) async-start(bf16[4,32,2048]{2,1,0:T(8,128)(2,1)} %shard_map.164), calls=%async_computation | async-start | bytes 1048576 | tf_op jit(solution)/shard_map/all_to_all | solution.py:470
  8.6 17.2 %copy-start.3 = (bf16[2,128,1024]{2,1,0:T(8,128)(2,1)}, bf16[2,128,1024]{2,1,0:T(8,128)(2,1)S(1)}, u32[]{:S(2)}) copy-start(bf16[2,128,1024]{2,1,0:T(8,128)(2,1)S(1)} %get-tuple-element.22.split_far) | copy-start | bytes 1572868
  25.8 28.4 %copy-start = (bf16[2048,256]{1,0:T(8,128)(2,1)S(1)}, bf16[2048,256]{1,0:T(8,128)(2,1)}, u32[]{:S(2)}) copy-start(bf16[2048,256]{1,0:T(8,128)(2,1)} %w_query.1) | copy-start | bytes 3145732
  52.3 61.7 %collective-permute-start.9 = (bf16[8,128,384]{2,1,0:T(8,128)(2,1)S(1)}, bf16[8,128,384]{2,1,0:T(8,128)(2,1)S(1)}, u32[]{:S(2)}, u32[]{:S(2)}) collective-permute-start(bf16[8,128,384]{2,1,0:T(8,128)(2,1)S(1)} %all_to_all.21), channel_id=1, source_target_pairs={{0,4},{4,0},{1,5},{5,1},{2,6},{6,2},{3,7},{7,3},{8,12},{12,8},{9,1... | collective-permute-start | bytes 2359304 | tf_op jit(solution)/shard_map/ppermute | solution.py:445
  58.7 12.9 %collective-permute-start = (bf16[400,128]{1,0:T(8,128)(2,1)S(1)}, bf16[400,128]{1,0:T(8,128)(2,1)S(1)}, u32[]{:S(2)}, u32[]{:S(2)}) collective-permute-start(bf16[400,128]{1,0:T(8,128)(2,1)S(1)} %get-tuple-element.24), channel_id=1, source_target_pairs={{0,32},{32,0},{1,33},{33,1},{2,34},{34,2},{3,35},{35,3},{4,36},{36... | collective-permute-start | bytes 307208 | tf_op jit(solution)/shard_map/ppermute | solution.py:445
  71.7 28.1 %copy-start.10 = (f32[2]{0:T(128)S(1)}, f32[2]{0:T(128)}, u32[]{:S(2)}) copy-start(f32[2]{0:T(128)} %mix.1) | copy-start | bytes 28
  71.7 28.0 %copy-start.11 = (f32[128]{0:T(128)S(1)}, f32[128]{0:T(128)}, u32[]{:S(2)}) copy-start(f32[128]{0:T(128)} %param.31) | copy-start | bytes 1540
  71.7 11.1 %collective-permute-start.5 = (bf16[544,128]{1,0:T(8,128)(2,1)S(1)}, bf16[544,128]{1,0:T(8,128)(2,1)S(1)}, u32[]{:S(2)}, u32[]{:S(2)}) collective-permute-start(bf16[544,128]{1,0:T(8,128)(2,1)S(1)} %shard_map.167), channel_id=1, source_target_pairs={{0,384},{64,448},{128,0},{1,385},{65,449},{129,1},{2,386},{66,450}... | collective-permute-start | bytes 417800 | tf_op jit(solution)/shard_map/ppermute | solution.py:537
  73.0 12.2 %collective-permute-start.2 = (bf16[544,128]{1,0:T(8,128)(2,1)S(1)}, bf16[544,128]{1,0:T(8,128)(2,1)S(1)}, u32[]{:S(2)}, u32[]{:S(2)}) collective-permute-start(bf16[544,128]{1,0:T(8,128)(2,1)S(1)} %shard_map.167), channel_id=1, source_target_pairs={{0,128},{64,192},{128,256},{192,320},{256,384},{320,448},{1,129},{... | collective-permute-start | bytes 417800 | tf_op jit(solution)/shard_map/ppermute | solution.py:537
  74.3 12.2 %collective-permute-start.7 = (bf16[544,128]{1,0:T(8,128)(2,1)S(1)}, bf16[544,128]{1,0:T(8,128)(2,1)S(1)}, u32[]{:S(2)}, u32[]{:S(2)}) collective-permute-start(bf16[544,128]{1,0:T(8,128)(2,1)S(1)} %shard_map.167), channel_id=1, source_target_pairs={{0,448},{1,449},{2,450},{3,451},{4,452},{5,453},{6,454},{7,455},{8... | collective-permute-start | bytes 417800 | tf_op jit(solution)/shard_map/ppermute | solution.py:537
  75.0 15.7 %collective-permute-start.1 = (bf16[544,128]{1,0:T(8,128)(2,1)S(1)}, bf16[544,128]{1,0:T(8,128)(2,1)S(1)}, u32[]{:S(2)}, u32[]{:S(2)}) collective-permute-start(bf16[544,128]{1,0:T(8,128)(2,1)S(1)} %shard_map.167), channel_id=1, source_target_pairs={{0,64},{64,128},{128,192},{192,256},{256,320},{320,384},{384,448},... | collective-permute-start | bytes 417800 | tf_op jit(solution)/shard_map/ppermute | solution.py:537
  82.8 7.9 %collective-permute-start.6 = (bf16[544,128]{1,0:T(8,128)(2,1)S(1)}, bf16[544,128]{1,0:T(8,128)(2,1)S(1)}, u32[]{:S(2)}, u32[]{:S(2)}) collective-permute-start(bf16[544,128]{1,0:T(8,128)(2,1)S(1)} %collective-permute-done.5.rest_5_), channel_id=1, source_target_pairs={{384,320},{448,384},{0,448},{385,321},{449,385},{1,449},{386,322},... | collective-permute-start | bytes 417800 | tf_op jit(solution)/shard_map/ppermute | solution.py:537
  85.2 10.2 %collective-permute-start.4 = (bf16[544,128]{1,0:T(8,128)(2,1)S(1)}, bf16[544,128]{1,0:T(8,128)(2,1)S(1)}, u32[]{:S(2)}, u32[]{:S(2)}) collective-permute-start(bf16[544,128]{1,0:T(8,128)(2,1)S(1)} %collective-permute-done.2.rest_1_), channel_id=1, source_target_pairs={{128,256},{192,320},{256,384},{320,448},{129,257},{193,321},{257,3... | collective-permute-start | bytes 417800 | tf_op jit(solution)/shard_map/ppermute | solution.py:537
  86.5 13.2 %collective-permute-start.3 = (bf16[544,128]{1,0:T(8,128)(2,1)S(1)}, bf16[544,128]{1,0:T(8,128)(2,1)S(1)}, u32[]{:S(2)}, u32[]{:S(2)}) collective-permute-start(bf16[544,128]{1,0:T(8,128)(2,1)S(1)} %collective-permute-done.2.rest_1_), channel_id=1, source_target_pairs={{128,192},{192,256},{256,320},{320,384},{384,448},{129,193},{193,2... | collective-permute-start | bytes 417800 | tf_op jit(solution)/shard_map/ppermute | solution.py:537
  99.7 7.8 %copy-start.5 = (f32[2,8,16,64]{3,2,1,0:T(8,128)S(1)}, f32[2,8,16,64]{3,2,1,0:T(8,128)}, u32[]{:S(2)}) copy-start(f32[2,8,16,64]{3,2,1,0:T(8,128)} %param.27) | copy-start | bytes 196612
  99.7 7.8 %copy-start.6 = (f32[8,2,8,64]{3,2,1,0:T(8,128)S(1)}, f32[8,2,8,64]{3,2,1,0:T(8,128)}, u32[]{:S(2)}) copy-start(f32[8,2,8,64]{3,2,1,0:T(8,128)} %init.1) | copy-start | bytes 98308
  104.2 3.3 %copy-start.9 = (f32[8,16]{1,0:T(8,128)S(1)}, f32[8,16]{1,0:T(8,128)}, u32[]{:S(2)}) copy-start(f32[8,16]{1,0:T(8,128)} %skip.1) | copy-start | bytes 1540
  104.2 9.7 %collective-permute-start.8 = (bf16[128,128]{1,0:T(8,128)(2,1)S(1)}, bf16[128,128]{1,0:T(8,128)(2,1)S(1)}, u32[]{:S(2)}, u32[]{:S(2)}) collective-permute-start(bf16[128,128]{1,0:T(8,128)(2,1)S(1)} %get-tuple-element.29), channel_id=1, source_target_pairs={{0,32},{32,0},{1,33},{33,1},{2,34},{34,2},{3,35},{35,3},{4,36},{36... | collective-permute-start | bytes 98312 | tf_op jit(solution)/shard_map/ppermute | solution.py:445
  (3 other events, 2.4 us)

commit v2 on v1

--- a/solution.py
+++ b/solution.py
@@ -158,8 +158,8 @@
 def project_kernel(
     place,
     tokens,
-    gain,
     w_query,
+    gain_far,
     w_key_far,
     tables_far,
     w_state_far,
@@ -169,6 +169,7 @@
     keep,
     send,
     drive_far,
+    gain,
     w_key,
     tables,
     w_state,
@@ -178,8 +179,8 @@
     drive_near,
     arrived,
 ):
-    far = (w_key_far, tables_far, w_state_far, split_far, trans_far, w_value_far)
-    near = (w_key, tables, w_state, in_split, trans, w_value)
+    far = (gain_far, w_state_far, split_far, tables_far, trans_far, w_key_far, w_value_far)
+    near = (gain, w_state, in_split, tables, trans, w_key, w_value)
     copies = [
         pltpu.make_async_copy(source, target, arrived.at[i])
         for i, (source, target) in enumerate(zip(far, near))
@@ -189,6 +190,7 @@
     head = place[1]
     wide = tokens[...].astype(f32)
     scale = lax.rsqrt(jnp.mean(wide * wide, axis=-1, keepdims=True) + EPSILON)
+    copies[0].wait()
     normed = (wide * scale * gain[...]).astype(bf16)
 
     def put(at, first, second):
@@ -197,9 +199,7 @@
         send[place_rows, :] = jnp.where(head == 0, second, first)
 
     query = dot(normed, w_query[...])
-    copies[0].wait()
-    key = dot(normed, w_key[...])
-    for copy in copies[1:5]:
+    for copy in copies[1:4]:
         copy.wait()
     lane = lax.broadcasted_iota(jnp.int32, (ROWS, LANES), 1)
     first_half = lane % QK_DIM < QK_DIM // 2
@@ -216,18 +216,20 @@
     drive = dot(normed, w_state[...]).astype(bf16)
     ordered = dot(row_order(False).astype(bf16), drive).astype(bf16)
     drive_near[...] = ordered
-    put(0, turned(key[:, :LANES]), turned(key[:, LANES:]))
     put(
         2,
         turned(query[:, :LANES]) * QK_DIM**-0.5,
         turned(query[:, LANES:]) * QK_DIM**-0.5,
     )
+    for copy in copies[4:]:
+        copy.wait()
+    leaving = pltpu.make_async_copy(drive_near, drive_far, arrived.at[7])
+    leaving.start()
     inject = inject_of(ordered, in_split)
-    copies[5].wait()
-    leaving = pltpu.make_async_copy(drive_near, drive_far, arrived.at[6])
-    leaving.start()
+    key = dot(normed, w_key[...])
     value = dot(normed, w_value[...])
     put(1, value[:, :LANES].astype(bf16), value[:, LANES:].astype(bf16))
+    put(0, turned(key[:, :LANES]), turned(key[:, LANES:]))
     _, element_parts = scan_blocks(
         inject,
         trans,
@@ -508,8 +510,8 @@
         (
             place,
             gathered,
-            norm_gain.reshape(1, -1),
             w_query,
+            in_hbm(norm_gain.reshape(1, -1)),
             in_hbm(w_key),
             in_hbm(tables),
             in_hbm(w_state_in),
@@ -518,6 +520,7 @@
             in_hbm(w_value),
         ),
         [
+            pltpu.VMEM((1, tokens.shape[1]), f32),
             pltpu.VMEM(w_key.shape, bf16),
             pltpu.VMEM(tables.shape, f32),
             pltpu.VMEM(w_state_in.shape, bf16),
@@ -525,9 +528,9 @@
             pltpu.VMEM(trans.shape, f32),
             pltpu.VMEM(w_value.shape, bf16),
             pltpu.VMEM((ROWS, GROUPS * GROUP), bf16),
-            pltpu.SemaphoreType.DMA((7,)),
+            pltpu.SemaphoreType.DMA((8,)),
         ],
-        far=6,
+        far=7,
         far_out=1,
     )
     got = swapped(send, "h")

time: 127 us -> 126 us (level)
    unnamed x33 -> x31, local copies, waits for them, and re-layouts: 3.13 us -> 2.53 us
where the time goes in v2:
time: 126 us; the launch traced here: 125 us
  blocking collectives  47 us (37%)
  waiting for transfers between devices  33.5 us (27%)
  starting transfers between devices  27.2 us (22%)
  Pallas kernels  13 us (10%)
  local copies, waits for them, and re-layouts  2.53 us (2%)
  other arithmetic  1.85 us (1%)
    all_to_all x1, blocking collectives, local(): weight_blocks = lax.all_to_all(fanned(weight_rows, Y), Y, 0, 0, tiled=True)  26.3 us
    ppermute x7, starting transfers between devices, along(): return lax.ppermute(x, 'z', pairs)  14.2 us
    ppermute x7, waiting for transfers between devices, along(): return lax.ppermute(x, 'z', pairs)  13.7 us
    ppermute x3, waiting for transfers between devices, swapped(): return lax.ppermute(x, axis, [(0, 1), (1, 0)])  13.7 us
    pallas_call x9, Pallas kernels, call(): pl.pallas_call(body, out_shape=[jax.ShapeDtypeStruct(s, d) for s, d in ou...  13 us
    all_to_all x1, blocking collectives, local(): shares = lax.all_to_all(parts, 'tp', 0, 0, tiled=True)  10.5 us
    all_to_all x1, blocking collectives, local(): weight_rows = lax.all_to_all(fan_weights, 'z', 0, 0, tiled=True)  10.2 us
    ppermute x3, starting transfers between devices, swapped(): return lax.ppermute(x, axis, [(0, 1), (1, 0)])  8.55 us
  transfers between devices with their start and end apart: 11, of which 7 were waited for; matrix products, arithmetic and copies ran while one was open for 1% of the time, Pallas kernels for 9%

profile of v2, /device:TPU:392, one launch (start us, length us, event | category | flops | bytes accessed | tf_op | source)
XLA Modules:
  0.0 125.4 jit_solution(7515013875199602697)
XLA Ops:
  0.0 0.9 copy-done.4
  1.8 4.4 %all-to-all-start = ((bf16[4,32,2048]{2,1,0:T(8,128)(2,1)}), bf16[4,32,2048]{2,1,0:T(8,128)(2,1)S(1)}, u32[]{:S(2)}, u32[]{:S(2)}) async-start(bf16[4,32,2048]{2,1,0:T(8,128)(2,1)} %shard_map.164), calls=%async_computation | async-start | bytes 1048576 | tf_op jit(solution)/shard_map/all_to_all | solution.py:472
  9.6 6.1 %all-to-all-done = bf16[4,32,2048]{2,1,0:T(8,128)(2,1)S(1)} async-done(((bf16[4,32,2048]{2,1,0:T(8,128)(2,1)}), bf16[4,32,2048]{2,1,0:T(8,128)(2,1)S(1)}, u32[]{:S(2)}, u32[]{:S(2)}) %all-to-all-start) | async-done | bytes 524320 | tf_op jit(solution)/shard_map/all_to_all | solution.py:472
  15.7 10.2 %all_to_all.20 = bf16[8,16,384]{2,1,0:T(8,128)(2,1)S(1)} all-to-all(bf16[8,16,384]{2,1,0:T(8,128)(2,1)S(1)} %shard_map.163), channel_id=1, replica_groups=mesh['z'=8,'h'=2,'q'=4,'c'=2,'tp'=4] {'z'}, dimensions={0} | all-to-all | bytes 196608 | tf_op jit(solution)/shard_map/all_to_all | solution.py:502
  25.9 26.3 %all_to_all.21 = bf16[8,128,384]{2,1,0:T(8,128)(2,1)S(1)} all-to-all(bf16[8,128,384]{2,1,0:T(8,128)(2,1)S(1)} %shard_map.170), channel_id=1, replica_groups=mesh['z'=8,'h'=2,'q'=4,'c'=2,'tp'=4] {'h','q'}, dimensions={0} | all-to-all | bytes 1572864 | tf_op jit(solution)/shard_map/all_to_all | solution.py:551
  52.3 1.9 %collective-permute-start.9 = (bf16[8,128,384]{2,1,0:T(8,128)(2,1)S(1)}, bf16[8,128,384]{2,1,0:T(8,128)(2,1)S(1)}, u32[]{:S(2)}, u32[]{:S(2)}) collective-permute-start(bf16[8,128,384]{2,1,0:T(8,128)(2,1)S(1)} %all_to_all.21), channel_id=1, source_target_pairs={{0,4},{4,0},{1,5},{5,1},{2,6},{6,2},{3,7},{7,3},{8,12},{12,8},{9,1... | collective-permute-start | bytes 2359304 | tf_op jit(solution)/shard_map/ppermute | solution.py:447
  54.3 3.5 %shard_map.166 = (bf16[400,128]{1,0:T(8,128)(2,1)S(1)}, bf16[400,128]{1,0:T(8,128)(2,1)S(1)}, bf16[128,128]{1,0:T(8,128)(2,1)S(1)}) custom-call(s32[4]{0:T(128)S(1)} %pad_add_fusion.place, bf16[128,2048]{1,0:T(8,128)(2,1)S(1)} %bitcast.19, bf16[2048,256]{1,0:T(8,128)(2,1)S(1)} %copy-done, f32[1,2048]{1,0:T(1,128)} %bitcast.26, bf16[2048,256]{1,0:T(8,128)(2,1)} %w_key_far.1, ...), custom_call_target="tpu_custom_call" | custom-call | tf_op jit(solution)/shard_map/pallas_call | solution.py:426
  57.8 3.4 %collective-permute-start = (bf16[400,128]{1,0:T(8,128)(2,1)S(1)}, bf16[400,128]{1,0:T(8,128)(2,1)S(1)}, u32[]{:S(2)}, u32[]{:S(2)}) collective-permute-start(bf16[400,128]{1,0:T(8,128)(2,1)S(1)} %get-tuple-element.24), channel_id=1, source_target_pairs={{0,32},{32,0},{1,33},{33,1},{2,34},{34,2},{3,35},{35,3},{4,36},{36... | collective-permute-start | bytes 307208 | tf_op jit(solution)/shard_map/ppermute | solution.py:447
  61.1 9.6 %collective-permute-done.got = bf16[400,128]{1,0:T(8,128)(2,1)S(1)} collective-permute-done((bf16[400,128]{1,0:T(8,128)(2,1)S(1)}, bf16[400,128]{1,0:T(8,128)(2,1)S(1)}, u32[]{:S(2)}, u32[]{:S(2)}) %collective-permute-start) | collective-permute-done | bytes 102432 | tf_op jit(solution)/shard_map/ppermute | solution.py:447
  70.7 1.3 %collective-permute-start.5 = (bf16[544,128]{1,0:T(8,128)(2,1)S(1)}, bf16[544,128]{1,0:T(8,128)(2,1)S(1)}, u32[]{:S(2)}, u32[]{:S(2)}) collective-permute-start(bf16[544,128]{1,0:T(8,128)(2,1)S(1)} %shard_map.167), channel_id=1, source_target_pairs={{0,384},{64,448},{128,0},{1,385},{65,449},{129,1},{2,386},{66,450}... | collective-permute-start | bytes 417800 | tf_op jit(solution)/shard_map/ppermute | solution.py:540
  72.0 1.3 %collective-permute-start.2 = (bf16[544,128]{1,0:T(8,128)(2,1)S(1)}, bf16[544,128]{1,0:T(8,128)(2,1)S(1)}, u32[]{:S(2)}, u32[]{:S(2)}) collective-permute-start(bf16[544,128]{1,0:T(8,128)(2,1)S(1)} %shard_map.167), channel_id=1, source_target_pairs={{0,128},{64,192},{128,256},{192,320},{256,384},{320,448},{1,129},{... | collective-permute-start | bytes 417800 | tf_op jit(solution)/shard_map/ppermute | solution.py:540
  74.0 3.6 %collective-permute-start.1 = (bf16[544,128]{1,0:T(8,128)(2,1)S(1)}, bf16[544,128]{1,0:T(8,128)(2,1)S(1)}, u32[]{:S(2)}, u32[]{:S(2)}) collective-permute-start(bf16[544,128]{1,0:T(8,128)(2,1)S(1)} %shard_map.167), channel_id=1, source_target_pairs={{0,64},{64,128},{128,192},{192,256},{256,320},{320,384},{384,448},... | collective-permute-start | bytes 417800 | tf_op jit(solution)/shard_map/ppermute | solution.py:540
  77.6 4.3 %collective-permute-done.5.rest_5_ = bf16[544,128]{1,0:T(8,128)(2,1)S(1)} collective-permute-done((bf16[544,128]{1,0:T(8,128)(2,1)S(1)}, bf16[544,128]{1,0:T(8,128)(2,1)S(1)}, u32[]{:S(2)}, u32[]{:S(2)}) %collective-permute-start.5) | collective-permute-done | bytes 139296 | tf_op jit(solution)/shard_map/ppermute | solution.py:540
  81.9 1.9 %collective-permute-start.6 = (bf16[544,128]{1,0:T(8,128)(2,1)S(1)}, bf16[544,128]{1,0:T(8,128)(2,1)S(1)}, u32[]{:S(2)}, u32[]{:S(2)}) collective-permute-start(bf16[544,128]{1,0:T(8,128)(2,1)S(1)} %collective-permute-done.5.rest_5_), channel_id=1, source_target_pairs={{384,320},{448,384},{0,448},{385,321},{449,385},{1,449},{386,322},... | collective-permute-start | bytes 417800 | tf_op jit(solution)/shard_map/ppermute | solution.py:540
  84.2 1.3 %collective-permute-start.4 = (bf16[544,128]{1,0:T(8,128)(2,1)S(1)}, bf16[544,128]{1,0:T(8,128)(2,1)S(1)}, u32[]{:S(2)}, u32[]{:S(2)}) collective-permute-start(bf16[544,128]{1,0:T(8,128)(2,1)S(1)} %collective-permute-done.2.rest_1_), channel_id=1, source_target_pairs={{128,256},{192,320},{256,384},{320,448},{129,257},{193,321},{257,3... | collective-permute-start | bytes 417800 | tf_op jit(solution)/shard_map/ppermute | solution.py:540
  85.5 4.2 %collective-permute-start.3 = (bf16[544,128]{1,0:T(8,128)(2,1)S(1)}, bf16[544,128]{1,0:T(8,128)(2,1)S(1)}, u32[]{:S(2)}, u32[]{:S(2)}) collective-permute-start(bf16[544,128]{1,0:T(8,128)(2,1)S(1)} %collective-permute-done.2.rest_1_), channel_id=1, source_target_pairs={{128,192},{192,256},{256,320},{320,384},{384,448},{129,193},{193,2... | collective-permute-start | bytes 417800 | tf_op jit(solution)/shard_map/ppermute | solution.py:540
  89.8 4.7 %collective-permute-done.4.rest_3_ = bf16[544,128]{1,0:T(8,128)(2,1)S(1)} collective-permute-done((bf16[544,128]{1,0:T(8,128)(2,1)S(1)}, bf16[544,128]{1,0:T(8,128)(2,1)S(1)}, u32[]{:S(2)}, u32[]{:S(2)}) %collective-permute-start.4) | collective-permute-done | bytes 139296 | tf_op jit(solution)/shard_map/ppermute | solution.py:540
  94.5 4.3 %collective-permute-done.3.rest_2_ = bf16[544,128]{1,0:T(8,128)(2,1)S(1)} collective-permute-done((bf16[544,128]{1,0:T(8,128)(2,1)S(1)}, bf16[544,128]{1,0:T(8,128)(2,1)S(1)}, u32[]{:S(2)}, u32[]{:S(2)}) %collective-permute-start.3) | collective-permute-done | bytes 139296 | tf_op jit(solution)/shard_map/ppermute | solution.py:540
  98.8 4.4 %shard_map.168 = (bf16[128,128]{1,0:T(8,128)(2,1)S(1)}, bf16[128,128]{1,0:T(8,128)(2,1)S(1)}, bf16[224,128]{1,0:T(8,128)(2,1)S(1)}) custom-call(s32[4]{0:T(128)S(1)} %pad_add_fusion.place, f32[2]{0:T(128)S(1)} %copy-done.9, f32[1,128]{1,0:T(1,128)S(1)} %bitcast.25, bf16[400,128]{1,0:T(8,128)(2,1)S(1)} %get-tuple-element.25.keep, ...), custom_call_target="tpu_custom_call" | custom-call | tf_op jit(solution)/shard_map/pallas_call | solution.py:426
  103.3 3.3 %collective-permute-start.8 = (bf16[128,128]{1,0:T(8,128)(2,1)S(1)}, bf16[128,128]{1,0:T(8,128)(2,1)S(1)}, u32[]{:S(2)}, u32[]{:S(2)}) collective-permute-start(bf16[128,128]{1,0:T(8,128)(2,1)S(1)} %get-tuple-element.29), channel_id=1, source_target_pairs={{0,32},{32,0},{1,33},{33,1},{2,34},{34,2},{3,35},{35,3},{4,36},{36... | collective-permute-start | bytes 98312 | tf_op jit(solution)/shard_map/ppermute | solution.py:447
  106.6 2.3 %shard_map.169.state = bf16[128,128]{1,0:T(8,128)(2,1)S(1)} custom-call(s32[4]{0:T(128)S(1)} %pad_add_fusion.place, f32[8,2,8,64]{3,2,1,0:T(8,128)S(1)} %copy-done.6, bf16[400,128]{1,0:T(8,128)(2,1)S(1)} %collective-permute-done.got, bf16[224,128]{1,0:T(8,128)(2,1)S(1)} %get-tuple-element.26.elements, bf16[128,128]{1,0:T(8,128)(2,1)S(1)} %get-tuple-element.27.drive, ...), custom_call_target="tpu_custom_call" | custom-call | tf_op jit(solution)/shard_map/pallas_call | solution.py:426
  108.8 4.1 %collective-permute-done.8.came = bf16[128,128]{1,0:T(8,128)(2,1)S(1)} collective-permute-done((bf16[128,128]{1,0:T(8,128)(2,1)S(1)}, bf16[128,128]{1,0:T(8,128)(2,1)S(1)}, u32[]{:S(2)}, u32[]{:S(2)}) %collective-permute-start.8) | collective-permute-done | bytes 32800 | tf_op jit(solution)/shard_map/ppermute | solution.py:447
  113.0 1.2 shard_map.171
  114.2 10.5 %all_to_all.22 = bf16[4,32,2048]{2,1,0:T(8,128)(2,1)S(1)} all-to-all(bf16[4,32,2048]{2,1,0:T(8,128)(2,1)S(1)} %bitcast.18), channel_id=1, replica_groups=mesh['z'=8,'h'=2,'q'=4,'c'=2,'tp'=4] {'tp'}, dimensions={0} | all-to-all | bytes 1048576 | tf_op jit(solution)/shard_map/all_to_all | solution.py:596
  (49 shorter events, 6.2 us)
Async XLA Ops:
  0.0 0.9 copy-start.4
  1.7 4.5 %copy-start.11 = (bf16[256,16]{0,1:T(8,128)(2,1)S(1)}, bf16[256,16]{0,1:T(8,128)(2,1)}, u32[]{:S(2)}) copy-start(bf16[256,16]{0,1:T(8,128)(2,1)} %param.33) | copy-start | bytes 24580
  1.7 4.5 %copy-start.14 = (bf16[128,16]{0,1:T(8,128)(2,1)S(1)}, bf16[128,16]{0,1:T(8,128)(2,1)}, u32[]{:S(2)}) copy-start(bf16[128,16]{0,1:T(8,128)(2,1)} %param.32) | copy-start | bytes 12292
  1.8 4.5 %copy-start.7 = (f32[8,64]{1,0:T(8,128)S(1)}, f32[8,64]{1,0:T(8,128)}, u32[]{:S(2)}) copy-start(f32[8,64]{1,0:T(8,128)} %decay.3) | copy-start | bytes 6148
  1.8 4.5 %copy-start.12 = (f32[8,64]{1,0:T(8,128)S(1)}, f32[8,64]{1,0:T(8,128)}, u32[]{:S(2)}) copy-start(f32[8,64]{1,0:T(8,128)} %param.24) | copy-start | bytes 6148
  1.8 4.6 %copy-start.13 = (f32[128,8]{0,1:T(8,128)S(1)}, f32[128,8]{0,1:T(8,128)}, u32[]{:S(2)}) copy-start(f32[128,8]{0,1:T(8,128)} %param.25) | copy-start | bytes 12292
  1.8 13.9 %all-to-all-start = ((bf16[4,32,2048]{2,1,0:T(8,128)(2,1)}), bf16[4,32,2048]{2,1,0:T(8,128)(2,1)S(1)}, u32[]{:S(2)}, u32[]{:S(2)}) async-start(bf16[4,32,2048]{2,1,0:T(8,128)(2,1)} %shard_map.164), calls=%async_computation | async-start | bytes 1048576 | tf_op jit(solution)/shard_map/all_to_all | solution.py:472
  8.6 17.2 %copy-start.3 = (bf16[2,128,1024]{2,1,0:T(8,128)(2,1)}, bf16[2,128,1024]{2,1,0:T(8,128)(2,1)S(1)}, u32[]{:S(2)}) copy-start(bf16[2,128,1024]{2,1,0:T(8,128)(2,1)S(1)} %get-tuple-element.22.split_far) | copy-start | bytes 1572868
  25.8 28.4 %copy-start = (bf16[2048,256]{1,0:T(8,128)(2,1)S(1)}, bf16[2048,256]{1,0:T(8,128)(2,1)}, u32[]{:S(2)}) copy-start(bf16[2048,256]{1,0:T(8,128)(2,1)} %w_query.1) | copy-start | bytes 3145732
  52.3 60.7 %collective-permute-start.9 = (bf16[8,128,384]{2,1,0:T(8,128)(2,1)S(1)}, bf16[8,128,384]{2,1,0:T(8,128)(2,1)S(1)}, u32[]{:S(2)}, u32[]{:S(2)}) collective-permute-start(bf16[8,128,384]{2,1,0:T(8,128)(2,1)S(1)} %all_to_all.21), channel_id=1, source_target_pairs={{0,4},{4,0},{1,5},{5,1},{2,6},{6,2},{3,7},{7,3},{8,12},{12,8},{9,1... | collective-permute-start | bytes 2359304 | tf_op jit(solution)/shard_map/ppermute | solution.py:447
  57.8 12.9 %collective-permute-start = (bf16[400,128]{1,0:T(8,128)(2,1)S(1)}, bf16[400,128]{1,0:T(8,128)(2,1)S(1)}, u32[]{:S(2)}, u32[]{:S(2)}) collective-permute-start(bf16[400,128]{1,0:T(8,128)(2,1)S(1)} %get-tuple-element.24), channel_id=1, source_target_pairs={{0,32},{32,0},{1,33},{33,1},{2,34},{34,2},{3,35},{35,3},{4,36},{36... | collective-permute-start | bytes 307208 | tf_op jit(solution)/shard_map/ppermute | solution.py:447
  70.7 28.1 %copy-start.9 = (f32[2]{0:T(128)S(1)}, f32[2]{0:T(128)}, u32[]{:S(2)}) copy-start(f32[2]{0:T(128)} %mix.1) | copy-start | bytes 28
  70.7 28.0 %copy-start.10 = (f32[128]{0:T(128)S(1)}, f32[128]{0:T(128)}, u32[]{:S(2)}) copy-start(f32[128]{0:T(128)} %param.31) | copy-start | bytes 1540
  70.7 11.1 %collective-permute-start.5 = (bf16[544,128]{1,0:T(8,128)(2,1)S(1)}, bf16[544,128]{1,0:T(8,128)(2,1)S(1)}, u32[]{:S(2)}, u32[]{:S(2)}) collective-permute-start(bf16[544,128]{1,0:T(8,128)(2,1)S(1)} %shard_map.167), channel_id=1, source_target_pairs={{0,384},{64,448},{128,0},{1,385},{65,449},{129,1},{2,386},{66,450}... | collective-permute-start | bytes 417800 | tf_op jit(solution)/shard_map/ppermute | solution.py:540
  72.0 12.2 %collective-permute-start.2 = (bf16[544,128]{1,0:T(8,128)(2,1)S(1)}, bf16[544,128]{1,0:T(8,128)(2,1)S(1)}, u32[]{:S(2)}, u32[]{:S(2)}) collective-permute-start(bf16[544,128]{1,0:T(8,128)(2,1)S(1)} %shard_map.167), channel_id=1, source_target_pairs={{0,128},{64,192},{128,256},{192,320},{256,384},{320,448},{1,129},{... | collective-permute-start | bytes 417800 | tf_op jit(solution)/shard_map/ppermute | solution.py:540
  73.3 12.2 %collective-permute-start.7 = (bf16[544,128]{1,0:T(8,128)(2,1)S(1)}, bf16[544,128]{1,0:T(8,128)(2,1)S(1)}, u32[]{:S(2)}, u32[]{:S(2)}) collective-permute-start(bf16[544,128]{1,0:T(8,128)(2,1)S(1)} %shard_map.167), channel_id=1, source_target_pairs={{0,448},{1,449},{2,450},{3,451},{4,452},{5,453},{6,454},{7,455},{8... | collective-permute-start | bytes 417800 | tf_op jit(solution)/shard_map/ppermute | solution.py:540
  74.0 15.7 %collective-permute-start.1 = (bf16[544,128]{1,0:T(8,128)(2,1)S(1)}, bf16[544,128]{1,0:T(8,128)(2,1)S(1)}, u32[]{:S(2)}, u32[]{:S(2)}) collective-permute-start(bf16[544,128]{1,0:T(8,128)(2,1)S(1)} %shard_map.167), channel_id=1, source_target_pairs={{0,64},{64,128},{128,192},{192,256},{256,320},{320,384},{384,448},... | collective-permute-start | bytes 417800 | tf_op jit(solution)/shard_map/ppermute | solution.py:540
  81.9 7.9 %collective-permute-start.6 = (bf16[544,128]{1,0:T(8,128)(2,1)S(1)}, bf16[544,128]{1,0:T(8,128)(2,1)S(1)}, u32[]{:S(2)}, u32[]{:S(2)}) collective-permute-start(bf16[544,128]{1,0:T(8,128)(2,1)S(1)} %collective-permute-done.5.rest_5_), channel_id=1, source_target_pairs={{384,320},{448,384},{0,448},{385,321},{449,385},{1,449},{386,322},... | collective-permute-start | bytes 417800 | tf_op jit(solution)/shard_map/ppermute | solution.py:540
  84.2 10.2 %collective-permute-start.4 = (bf16[544,128]{1,0:T(8,128)(2,1)S(1)}, bf16[544,128]{1,0:T(8,128)(2,1)S(1)}, u32[]{:S(2)}, u32[]{:S(2)}) collective-permute-start(bf16[544,128]{1,0:T(8,128)(2,1)S(1)} %collective-permute-done.2.rest_1_), channel_id=1, source_target_pairs={{128,256},{192,320},{256,384},{320,448},{129,257},{193,321},{257,3... | collective-permute-start | bytes 417800 | tf_op jit(solution)/shard_map/ppermute | solution.py:540
  85.5 13.2 %collective-permute-start.3 = (bf16[544,128]{1,0:T(8,128)(2,1)S(1)}, bf16[544,128]{1,0:T(8,128)(2,1)S(1)}, u32[]{:S(2)}, u32[]{:S(2)}) collective-permute-start(bf16[544,128]{1,0:T(8,128)(2,1)S(1)} %collective-permute-done.2.rest_1_), channel_id=1, source_target_pairs={{128,192},{192,256},{256,320},{320,384},{384,448},{129,193},{193,2... | collective-permute-start | bytes 417800 | tf_op jit(solution)/shard_map/ppermute | solution.py:540
  98.8 7.8 %copy-start.5 = (f32[2,8,16,64]{3,2,1,0:T(8,128)S(1)}, f32[2,8,16,64]{3,2,1,0:T(8,128)}, u32[]{:S(2)}) copy-start(f32[2,8,16,64]{3,2,1,0:T(8,128)} %param.27) | copy-start | bytes 196612
  98.8 7.8 %copy-start.6 = (f32[8,2,8,64]{3,2,1,0:T(8,128)S(1)}, f32[8,2,8,64]{3,2,1,0:T(8,128)}, u32[]{:S(2)}) copy-start(f32[8,2,8,64]{3,2,1,0:T(8,128)} %init.1) | copy-start | bytes 98308
  103.2 3.3 %copy-start.8 = (f32[8,16]{1,0:T(8,128)S(1)}, f32[8,16]{1,0:T(8,128)}, u32[]{:S(2)}) copy-start(f32[8,16]{1,0:T(8,128)} %skip.1) | copy-start | bytes 1540
  103.3 9.7 %collective-permute-start.8 = (bf16[128,128]{1,0:T(8,128)(2,1)S(1)}, bf16[128,128]{1,0:T(8,128)(2,1)S(1)}, u32[]{:S(2)}, u32[]{:S(2)}) collective-permute-start(bf16[128,128]{1,0:T(8,128)(2,1)S(1)} %get-tuple-element.29), channel_id=1, source_target_pairs={{0,32},{32,0},{1,33},{33,1},{2,34},{34,2},{3,35},{35,3},{4,36},{36... | collective-permute-start | bytes 98312 | tf_op jit(solution)/shard_map/ppermute | solution.py:447
  (2 other events, 1.7 us)

commit v3 on v2

--- a/solution.py
+++ b/solution.py
@@ -264,9 +264,11 @@
     for k in range(RING - 1):
         elements[2 * EL_ROWS * k : 2 * EL_ROWS * (k + 1), :] = passed[k][2 * pair :, :]
     query = jnp.concatenate([keep[2 * ROWS : 3 * ROWS, :], got[2 * ROWS : 3 * ROWS, :]], axis=0)
-    queries = (query[:, :QK_DIM], query[:, QK_DIM:])
-    row = lax.broadcasted_iota(jnp.int32, (pair, pair), 0)
-    column = lax.broadcasted_iota(jnp.int32, (pair, pair), 1)
+    low = lax.broadcasted_iota(jnp.int32, (pair, LANES), 1) < QK_DIM
+    zero = jnp.zeros_like(query)
+    both = jnp.concatenate([jnp.where(low, query, zero), jnp.where(low, zero, query)], axis=0)
+    row = lax.broadcasted_iota(jnp.int32, (2 * pair, pair), 0) % pair
+    column = lax.broadcasted_iota(jnp.int32, (2 * pair, pair), 1)
 
     def segment(index):
         block = jnp.where(index < ROWS, head, 1 - head)
@@ -275,37 +277,31 @@
     allowed = segment(column) <= segment(row)
     own_key = jnp.concatenate([keep[:ROWS, :], got[:ROWS, :]], axis=0)
     own_value = jnp.concatenate([keep[ROWS:pair, :], got[ROWS:pair, :]], axis=0)
-    for c in range(2):
-        raw = dot_nt(queries[c], own_key[:, c * QK_DIM : (c + 1) * QK_DIM])
-        masked = jnp.where(allowed, raw, MASK_FLOOR)
-        scores[c, 0] = masked
-        peak[c] = jnp.maximum(masked[:, :LANES], masked[:, LANES:])
+    masked = jnp.where(allowed, dot_nt(both, own_key), MASK_FLOOR)
+    scores[0] = masked
+    peak[...] = jnp.maximum(masked[:, :LANES], masked[:, LANES:])
     for k in range(1, RING):
 
         @pl.when(k <= depth)
         def _():
-            for c in range(2):
-                keys = passed[k - 1][:pair, c * QK_DIM : (c + 1) * QK_DIM]
-                raw = dot_nt(queries[c], keys)
-                scores[c, k] = raw
-                peak[c] = jnp.maximum(peak[c], jnp.maximum(raw[:, :LANES], raw[:, LANES:]))
-
-    tops = [jnp.max(peak[c], axis=-1, keepdims=True) for c in range(2)]
-    for c in range(2):
-        weight = jnp.exp(scores[c, 0] - tops[c])
-        total[c] = weight[:, :LANES] + weight[:, LANES:]
-        numerator[c] = dot(weight.astype(bf16), own_value)
+            raw = dot_nt(both, passed[k - 1][:pair, :])
+            scores[k] = raw
+            peak[...] = jnp.maximum(peak[...], jnp.maximum(raw[:, :LANES], raw[:, LANES:]))
+
+    top = jnp.max(peak[...], axis=-1, keepdims=True)
+    weight = jnp.exp(scores[0] - top)
+    total[...] = weight[:, :LANES] + weight[:, LANES:]
+    numerator[...] = dot(weight.astype(bf16), own_value)
     for k in range(1, RING):
 
         @pl.when(k <= depth)
         def _():
-            for c in range(2):
-                weight = jnp.exp(scores[c, k] - tops[c])
-                total[c] += weight[:, :LANES] + weight[:, LANES:]
-                numerator[c] += dot(weight.astype(bf16), passed[k - 1][pair : 2 * pair, :])
-
-    mapped = [numerator[c] / jnp.sum(total[c], axis=-1, keepdims=True) for c in range(2)]
-    difference = mapped[0] - mix[head] * mapped[1]
+            weight = jnp.exp(scores[k] - top)
+            total[...] += weight[:, :LANES] + weight[:, LANES:]
+            numerator[...] += dot(weight.astype(bf16), passed[k - 1][pair : 2 * pair, :])
+
+    mapped = numerator[...] / jnp.sum(total[...], axis=-1, keepdims=True)
+    difference = mapped[:pair] - mix[head] * mapped[pair:]
     mean = jnp.mean(difference * difference, axis=-1, keepdims=True)
     out = difference * lax.rsqrt(mean + EPSILON) * sub_gain[...] * (1.0 - LAMBDA_INIT)
     out_keep[...] = out[:ROWS].astype(bf16)
@@ -550,13 +546,13 @@
     passed = [one, two, three, four, five, six, seven]
     weight_blocks = lax.all_to_all(fanned(weight_rows, Y), Y, 0, 0, tiled=True)
 
-    pair = (2, 2 * ROWS, LANES)
+    pair = (4 * ROWS, LANES)
     out_keep, out_send, elements = call(
         attention_kernel,
         [((ROWS, LANES), bf16)] * 2 + [((2 * EL_ROWS * (RING - 1), LANES), bf16)],
         (0, 1),
         (place, mix_lambda, sub_gain.reshape(1, -1), keep, got, *passed),
-        [pltpu.VMEM((2, RING, 2 * ROWS, 2 * ROWS), f32)] + [pltpu.VMEM(pair, f32)] * 3,
+        [pltpu.VMEM((RING, 4 * ROWS, 2 * ROWS), f32)] + [pltpu.VMEM(pair, f32)] * 3,
     )
     came = swapped(out_send, "h")
 

time: 126 us -> 126 us (level)
  transfers between devices with their start and end apart: 11 -> 11, of which waited for: 7 -> 7; matrix products, arithmetic and copies ran while one was open for 1% -> 1% of each run, Pallas kernels for 9% -> 8%
where the time goes in v3:
time: 126 us; the launch traced here: 125 us
  blocking collectives  47 us (37%)
  waiting for transfers between devices  33.5 us (27%)
  starting transfers between devices  27.2 us (22%)
  Pallas kernels  12.7 us (10%)
  local copies, waits for them, and re-layouts  2.53 us (2%)
  other arithmetic  1.85 us (1%)
    all_to_all x1, blocking collectives, local(): weight_blocks = lax.all_to_all(fanned(weight_rows, Y), Y, 0, 0, tiled=True)  26.3 us
    ppermute x7, starting transfers between devices, along(): return lax.ppermute(x, 'z', pairs)  14.2 us
    ppermute x7, waiting for transfers between devices, along(): return lax.ppermute(x, 'z', pairs)  13.7 us
    ppermute x3, waiting for transfers between devices, swapped(): return lax.ppermute(x, axis, [(0, 1), (1, 0)])  13.7 us
    pallas_call x9, Pallas kernels, call(): pl.pallas_call(body, out_shape=[jax.ShapeDtypeStruct(s, d) for s, d in ou...  12.7 us
    all_to_all x1, blocking collectives, local(): shares = lax.all_to_all(parts, 'tp', 0, 0, tiled=True)  10.5 us
    all_to_all x1, blocking collectives, local(): weight_rows = lax.all_to_all(fan_weights, 'z', 0, 0, tiled=True)  10.2 us
    ppermute x3, starting transfers between devices, swapped(): return lax.ppermute(x, axis, [(0, 1), (1, 0)])  8.55 us
  transfers between devices with their start and end apart: 11, of which 7 were waited for; matrix products, arithmetic and copies ran while one was open for 1% of the time, Pallas kernels for 8%

profile of v3, /device:TPU:392, one launch (start us, length us, event | category | flops | bytes accessed | tf_op | source)
XLA Modules:
  0.0 125.1 jit_solution(8514863220347936699)
XLA Ops:
  0.0 0.9 copy-done.4
  1.8 4.4 %all-to-all-start = ((bf16[4,32,2048]{2,1,0:T(8,128)(2,1)}), bf16[4,32,2048]{2,1,0:T(8,128)(2,1)S(1)}, u32[]{:S(2)}, u32[]{:S(2)}) async-start(bf16[4,32,2048]{2,1,0:T(8,128)(2,1)} %shard_map.164), calls=%async_computation | async-start | bytes 1048576 | tf_op jit(solution)/shard_map/all_to_all | solution.py:468
  9.6 6.1 %all-to-all-done = bf16[4,32,2048]{2,1,0:T(8,128)(2,1)S(1)} async-done(((bf16[4,32,2048]{2,1,0:T(8,128)(2,1)}), bf16[4,32,2048]{2,1,0:T(8,128)(2,1)S(1)}, u32[]{:S(2)}, u32[]{:S(2)}) %all-to-all-start) | async-done | bytes 524320 | tf_op jit(solution)/shard_map/all_to_all | solution.py:468
  15.7 10.2 %all_to_all.20 = bf16[8,16,384]{2,1,0:T(8,128)(2,1)S(1)} all-to-all(bf16[8,16,384]{2,1,0:T(8,128)(2,1)S(1)} %shard_map.163), channel_id=1, replica_groups=mesh['z'=8,'h'=2,'q'=4,'c'=2,'tp'=4] {'z'}, dimensions={0} | all-to-all | bytes 196608 | tf_op jit(solution)/shard_map/all_to_all | solution.py:498
  25.9 26.3 %all_to_all.21 = bf16[8,128,384]{2,1,0:T(8,128)(2,1)S(1)} all-to-all(bf16[8,128,384]{2,1,0:T(8,128)(2,1)S(1)} %shard_map.170), channel_id=1, replica_groups=mesh['z'=8,'h'=2,'q'=4,'c'=2,'tp'=4] {'h','q'}, dimensions={0} | all-to-all | bytes 1572864 | tf_op jit(solution)/shard_map/all_to_all | solution.py:547
  52.3 1.9 %collective-permute-start.9 = (bf16[8,128,384]{2,1,0:T(8,128)(2,1)S(1)}, bf16[8,128,384]{2,1,0:T(8,128)(2,1)S(1)}, u32[]{:S(2)}, u32[]{:S(2)}) collective-permute-start(bf16[8,128,384]{2,1,0:T(8,128)(2,1)S(1)} %all_to_all.21), channel_id=1, source_target_pairs={{0,4},{4,0},{1,5},{5,1},{2,6},{6,2},{3,7},{7,3},{8,12},{12,8},{9,1... | collective-permute-start | bytes 2359304 | tf_op jit(solution)/shard_map/ppermute | solution.py:443
  54.3 3.5 %shard_map.166 = (bf16[400,128]{1,0:T(8,128)(2,1)S(1)}, bf16[400,128]{1,0:T(8,128)(2,1)S(1)}, bf16[128,128]{1,0:T(8,128)(2,1)S(1)}) custom-call(s32[4]{0:T(128)S(1)} %pad_add_fusion.place, bf16[128,2048]{1,0:T(8,128)(2,1)S(1)} %bitcast.19, bf16[2048,256]{1,0:T(8,128)(2,1)S(1)} %copy-done, f32[1,2048]{1,0:T(1,128)} %bitcast.26, bf16[2048,256]{1,0:T(8,128)(2,1)} %w_key_far.1, ...), custom_call_target="tpu_custom_call" | custom-call | tf_op jit(solution)/shard_map/pallas_call | solution.py:422
  57.8 3.4 %collective-permute-start = (bf16[400,128]{1,0:T(8,128)(2,1)S(1)}, bf16[400,128]{1,0:T(8,128)(2,1)S(1)}, u32[]{:S(2)}, u32[]{:S(2)}) collective-permute-start(bf16[400,128]{1,0:T(8,128)(2,1)S(1)} %get-tuple-element.24), channel_id=1, source_target_pairs={{0,32},{32,0},{1,33},{33,1},{2,34},{34,2},{3,35},{35,3},{4,36},{36... | collective-permute-start | bytes 307208 | tf_op jit(solution)/shard_map/ppermute | solution.py:443
  61.1 9.6 %collective-permute-done.got = bf16[400,128]{1,0:T(8,128)(2,1)S(1)} collective-permute-done((bf16[400,128]{1,0:T(8,128)(2,1)S(1)}, bf16[400,128]{1,0:T(8,128)(2,1)S(1)}, u32[]{:S(2)}, u32[]{:S(2)}) %collective-permute-start) | collective-permute-done | bytes 102432 | tf_op jit(solution)/shard_map/ppermute | solution.py:443
  70.7 1.3 %collective-permute-start.5 = (bf16[544,128]{1,0:T(8,128)(2,1)S(1)}, bf16[544,128]{1,0:T(8,128)(2,1)S(1)}, u32[]{:S(2)}, u32[]{:S(2)}) collective-permute-start(bf16[544,128]{1,0:T(8,128)(2,1)S(1)} %shard_map.167), channel_id=1, source_target_pairs={{0,384},{64,448},{128,0},{1,385},{65,449},{129,1},{2,386},{66,450}... | collective-permute-start | bytes 417800 | tf_op jit(solution)/shard_map/ppermute | solution.py:536
  72.0 1.3 %collective-permute-start.2 = (bf16[544,128]{1,0:T(8,128)(2,1)S(1)}, bf16[544,128]{1,0:T(8,128)(2,1)S(1)}, u32[]{:S(2)}, u32[]{:S(2)}) collective-permute-start(bf16[544,128]{1,0:T(8,128)(2,1)S(1)} %shard_map.167), channel_id=1, source_target_pairs={{0,128},{64,192},{128,256},{192,320},{256,384},{320,448},{1,129},{... | collective-permute-start | bytes 417800 | tf_op jit(solution)/shard_map/ppermute | solution.py:536
  74.0 3.6 %collective-permute-start.1 = (bf16[544,128]{1,0:T(8,128)(2,1)S(1)}, bf16[544,128]{1,0:T(8,128)(2,1)S(1)}, u32[]{:S(2)}, u32[]{:S(2)}) collective-permute-start(bf16[544,128]{1,0:T(8,128)(2,1)S(1)} %shard_map.167), channel_id=1, source_target_pairs={{0,64},{64,128},{128,192},{192,256},{256,320},{320,384},{384,448},... | collective-permute-start | bytes 417800 | tf_op jit(solution)/shard_map/ppermute | solution.py:536
  77.6 4.3 %collective-permute-done.5.rest_5_ = bf16[544,128]{1,0:T(8,128)(2,1)S(1)} collective-permute-done((bf16[544,128]{1,0:T(8,128)(2,1)S(1)}, bf16[544,128]{1,0:T(8,128)(2,1)S(1)}, u32[]{:S(2)}, u32[]{:S(2)}) %collective-permute-start.5) | collective-permute-done | bytes 139296 | tf_op jit(solution)/shard_map/ppermute | solution.py:536
  81.9 1.9 %collective-permute-start.6 = (bf16[544,128]{1,0:T(8,128)(2,1)S(1)}, bf16[544,128]{1,0:T(8,128)(2,1)S(1)}, u32[]{:S(2)}, u32[]{:S(2)}) collective-permute-start(bf16[544,128]{1,0:T(8,128)(2,1)S(1)} %collective-permute-done.5.rest_5_), channel_id=1, source_target_pairs={{384,320},{448,384},{0,448},{385,321},{449,385},{1,449},{386,322},... | collective-permute-start | bytes 417800 | tf_op jit(solution)/shard_map/ppermute | solution.py:536
  84.2 1.3 %collective-permute-start.4 = (bf16[544,128]{1,0:T(8,128)(2,1)S(1)}, bf16[544,128]{1,0:T(8,128)(2,1)S(1)}, u32[]{:S(2)}, u32[]{:S(2)}) collective-permute-start(bf16[544,128]{1,0:T(8,128)(2,1)S(1)} %collective-permute-done.2.rest_1_), channel_id=1, source_target_pairs={{128,256},{192,320},{256,384},{320,448},{129,257},{193,321},{257,3... | collective-permute-start | bytes 417800 | tf_op jit(solution)/shard_map/ppermute | solution.py:536
  85.5 4.2 %collective-permute-start.3 = (bf16[544,128]{1,0:T(8,128)(2,1)S(1)}, bf16[544,128]{1,0:T(8,128)(2,1)S(1)}, u32[]{:S(2)}, u32[]{:S(2)}) collective-permute-start(bf16[544,128]{1,0:T(8,128)(2,1)S(1)} %collective-permute-done.2.rest_1_), channel_id=1, source_target_pairs={{128,192},{192,256},{256,320},{320,384},{384,448},{129,193},{193,2... | collective-permute-start | bytes 417800 | tf_op jit(solution)/shard_map/ppermute | solution.py:536
  89.8 4.7 %collective-permute-done.4.rest_3_ = bf16[544,128]{1,0:T(8,128)(2,1)S(1)} collective-permute-done((bf16[544,128]{1,0:T(8,128)(2,1)S(1)}, bf16[544,128]{1,0:T(8,128)(2,1)S(1)}, u32[]{:S(2)}, u32[]{:S(2)}) %collective-permute-start.4) | collective-permute-done | bytes 139296 | tf_op jit(solution)/shard_map/ppermute | solution.py:536
  94.5 4.3 %collective-permute-done.3.rest_2_ = bf16[544,128]{1,0:T(8,128)(2,1)S(1)} collective-permute-done((bf16[544,128]{1,0:T(8,128)(2,1)S(1)}, bf16[544,128]{1,0:T(8,128)(2,1)S(1)}, u32[]{:S(2)}, u32[]{:S(2)}) %collective-permute-start.3) | collective-permute-done | bytes 139296 | tf_op jit(solution)/shard_map/ppermute | solution.py:536
  98.8 4.1 %shard_map.168 = (bf16[128,128]{1,0:T(8,128)(2,1)S(1)}, bf16[128,128]{1,0:T(8,128)(2,1)S(1)}, bf16[224,128]{1,0:T(8,128)(2,1)S(1)}) custom-call(s32[4]{0:T(128)S(1)} %pad_add_fusion.place, f32[2]{0:T(128)S(1)} %copy-done.9, f32[1,128]{1,0:T(1,128)S(1)} %bitcast.25, bf16[400,128]{1,0:T(8,128)(2,1)S(1)} %get-tuple-element.25.keep, ...), custom_call_target="tpu_custom_call" | custom-call | tf_op jit(solution)/shard_map/pallas_call | solution.py:422
  102.9 3.3 %collective-permute-start.8 = (bf16[128,128]{1,0:T(8,128)(2,1)S(1)}, bf16[128,128]{1,0:T(8,128)(2,1)S(1)}, u32[]{:S(2)}, u32[]{:S(2)}) collective-permute-start(bf16[128,128]{1,0:T(8,128)(2,1)S(1)} %get-tuple-element.29), channel_id=1, source_target_pairs={{0,32},{32,0},{1,33},{33,1},{2,34},{34,2},{3,35},{35,3},{4,36},{36... | collective-permute-start | bytes 98312 | tf_op jit(solution)/shard_map/ppermute | solution.py:443
  106.3 2.3 %shard_map.169.state = bf16[128,128]{1,0:T(8,128)(2,1)S(1)} custom-call(s32[4]{0:T(128)S(1)} %pad_add_fusion.place, f32[8,2,8,64]{3,2,1,0:T(8,128)S(1)} %copy-done.6, bf16[400,128]{1,0:T(8,128)(2,1)S(1)} %collective-permute-done.got, bf16[224,128]{1,0:T(8,128)(2,1)S(1)} %get-tuple-element.26.elements, bf16[128,128]{1,0:T(8,128)(2,1)S(1)} %get-tuple-element.27.drive, ...), custom_call_target="tpu_custom_call" | custom-call | tf_op jit(solution)/shard_map/pallas_call | solution.py:422
  108.5 4.1 %collective-permute-done.8.came = bf16[128,128]{1,0:T(8,128)(2,1)S(1)} collective-permute-done((bf16[128,128]{1,0:T(8,128)(2,1)S(1)}, bf16[128,128]{1,0:T(8,128)(2,1)S(1)}, u32[]{:S(2)}, u32[]{:S(2)}) %collective-permute-start.8) | collective-permute-done | bytes 32800 | tf_op jit(solution)/shard_map/ppermute | solution.py:443
  112.7 1.2 shard_map.171
  113.9 10.5 %all_to_all.22 = bf16[4,32,2048]{2,1,0:T(8,128)(2,1)S(1)} all-to-all(bf16[4,32,2048]{2,1,0:T(8,128)(2,1)S(1)} %bitcast.18), channel_id=1, replica_groups=mesh['z'=8,'h'=2,'q'=4,'c'=2,'tp'=4] {'tp'}, dimensions={0} | all-to-all | bytes 1048576 | tf_op jit(solution)/shard_map/all_to_all | solution.py:592
  (49 shorter events, 6.2 us)
Async XLA Ops:
  0.0 0.9 copy-start.4
  1.7 4.5 %copy-start.11 = (bf16[256,16]{0,1:T(8,128)(2,1)S(1)}, bf16[256,16]{0,1:T(8,128)(2,1)}, u32[]{:S(2)}) copy-start(bf16[256,16]{0,1:T(8,128)(2,1)} %param.33) | copy-start | bytes 24580
  1.7 4.5 %copy-start.14 = (bf16[128,16]{0,1:T(8,128)(2,1)S(1)}, bf16[128,16]{0,1:T(8,128)(2,1)}, u32[]{:S(2)}) copy-start(bf16[128,16]{0,1:T(8,128)(2,1)} %param.32) | copy-start | bytes 12292
  1.8 4.5 %copy-start.7 = (f32[8,64]{1,0:T(8,128)S(1)}, f32[8,64]{1,0:T(8,128)}, u32[]{:S(2)}) copy-start(f32[8,64]{1,0:T(8,128)} %decay.3) | copy-start | bytes 6148
  1.8 4.5 %copy-start.12 = (f32[8,64]{1,0:T(8,128)S(1)}, f32[8,64]{1,0:T(8,128)}, u32[]{:S(2)}) copy-start(f32[8,64]{1,0:T(8,128)} %param.24) | copy-start | bytes 6148
  1.8 4.6 %copy-start.13 = (f32[128,8]{0,1:T(8,128)S(1)}, f32[128,8]{0,1:T(8,128)}, u32[]{:S(2)}) copy-start(f32[128,8]{0,1:T(8,128)} %param.25) | copy-start | bytes 12292
  1.8 13.9 %all-to-all-start = ((bf16[4,32,2048]{2,1,0:T(8,128)(2,1)}), bf16[4,32,2048]{2,1,0:T(8,128)(2,1)S(1)}, u32[]{:S(2)}, u32[]{:S(2)}) async-start(bf16[4,32,2048]{2,1,0:T(8,128)(2,1)} %shard_map.164), calls=%async_computation | async-start | bytes 1048576 | tf_op jit(solution)/shard_map/all_to_all | solution.py:468
  8.6 17.2 %copy-start.3 = (bf16[2,128,1024]{2,1,0:T(8,128)(2,1)}, bf16[2,128,1024]{2,1,0:T(8,128)(2,1)S(1)}, u32[]{:S(2)}) copy-start(bf16[2,128,1024]{2,1,0:T(8,128)(2,1)S(1)} %get-tuple-element.22.split_far) | copy-start | bytes 1572868
  25.8 28.4 %copy-start = (bf16[2048,256]{1,0:T(8,128)(2,1)S(1)}, bf16[2048,256]{1,0:T(8,128)(2,1)}, u32[]{:S(2)}) copy-start(bf16[2048,256]{1,0:T(8,128)(2,1)} %w_query.1) | copy-start | bytes 3145732
  52.3 60.4 %collective-permute-start.9 = (bf16[8,128,384]{2,1,0:T(8,128)(2,1)S(1)}, bf16[8,128,384]{2,1,0:T(8,128)(2,1)S(1)}, u32[]{:S(2)}, u32[]{:S(2)}) collective-permute-start(bf16[8,128,384]{2,1,0:T(8,128)(2,1)S(1)} %all_to_all.21), channel_id=1, source_target_pairs={{0,4},{4,0},{1,5},{5,1},{2,6},{6,2},{3,7},{7,3},{8,12},{12,8},{9,1... | collective-permute-start | bytes 2359304 | tf_op jit(solution)/shard_map/ppermute | solution.py:443
  57.8 12.9 %collective-permute-start = (bf16[400,128]{1,0:T(8,128)(2,1)S(1)}, bf16[400,128]{1,0:T(8,128)(2,1)S(1)}, u32[]{:S(2)}, u32[]{:S(2)}) collective-permute-start(bf16[400,128]{1,0:T(8,128)(2,1)S(1)} %get-tuple-element.24), channel_id=1, source_target_pairs={{0,32},{32,0},{1,33},{33,1},{2,34},{34,2},{3,35},{35,3},{4,36},{36... | collective-permute-start | bytes 307208 | tf_op jit(solution)/shard_map/ppermute | solution.py:443
  70.7 28.1 %copy-start.9 = (f32[2]{0:T(128)S(1)}, f32[2]{0:T(128)}, u32[]{:S(2)}) copy-start(f32[2]{0:T(128)} %mix.1) | copy-start | bytes 28
  70.7 28.0 %copy-start.10 = (f32[128]{0:T(128)S(1)}, f32[128]{0:T(128)}, u32[]{:S(2)}) copy-start(f32[128]{0:T(128)} %param.31) | copy-start | bytes 1540
  70.7 11.1 %collective-permute-start.5 = (bf16[544,128]{1,0:T(8,128)(2,1)S(1)}, bf16[544,128]{1,0:T(8,128)(2,1)S(1)}, u32[]{:S(2)}, u32[]{:S(2)}) collective-permute-start(bf16[544,128]{1,0:T(8,128)(2,1)S(1)} %shard_map.167), channel_id=1, source_target_pairs={{0,384},{64,448},{128,0},{1,385},{65,449},{129,1},{2,386},{66,450}... | collective-permute-start | bytes 417800 | tf_op jit(solution)/shard_map/ppermute | solution.py:536
  72.0 12.2 %collective-permute-start.2 = (bf16[544,128]{1,0:T(8,128)(2,1)S(1)}, bf16[544,128]{1,0:T(8,128)(2,1)S(1)}, u32[]{:S(2)}, u32[]{:S(2)}) collective-permute-start(bf16[544,128]{1,0:T(8,128)(2,1)S(1)} %shard_map.167), channel_id=1, source_target_pairs={{0,128},{64,192},{128,256},{192,320},{256,384},{320,448},{1,129},{... | collective-permute-start | bytes 417800 | tf_op jit(solution)/shard_map/ppermute | solution.py:536
  73.3 12.2 %collective-permute-start.7 = (bf16[544,128]{1,0:T(8,128)(2,1)S(1)}, bf16[544,128]{1,0:T(8,128)(2,1)S(1)}, u32[]{:S(2)}, u32[]{:S(2)}) collective-permute-start(bf16[544,128]{1,0:T(8,128)(2,1)S(1)} %shard_map.167), channel_id=1, source_target_pairs={{0,448},{1,449},{2,450},{3,451},{4,452},{5,453},{6,454},{7,455},{8... | collective-permute-start | bytes 417800 | tf_op jit(solution)/shard_map/ppermute | solution.py:536
  74.0 15.7 %collective-permute-start.1 = (bf16[544,128]{1,0:T(8,128)(2,1)S(1)}, bf16[544,128]{1,0:T(8,128)(2,1)S(1)}, u32[]{:S(2)}, u32[]{:S(2)}) collective-permute-start(bf16[544,128]{1,0:T(8,128)(2,1)S(1)} %shard_map.167), channel_id=1, source_target_pairs={{0,64},{64,128},{128,192},{192,256},{256,320},{320,384},{384,448},... | collective-permute-start | bytes 417800 | tf_op jit(solution)/shard_map/ppermute | solution.py:536
  81.9 7.9 %collective-permute-start.6 = (bf16[544,128]{1,0:T(8,128)(2,1)S(1)}, bf16[544,128]{1,0:T(8,128)(2,1)S(1)}, u32[]{:S(2)}, u32[]{:S(2)}) collective-permute-start(bf16[544,128]{1,0:T(8,128)(2,1)S(1)} %collective-permute-done.5.rest_5_), channel_id=1, source_target_pairs={{384,320},{448,384},{0,448},{385,321},{449,385},{1,449},{386,322},... | collective-permute-start | bytes 417800 | tf_op jit(solution)/shard_map/ppermute | solution.py:536
  84.2 10.2 %collective-permute-start.4 = (bf16[544,128]{1,0:T(8,128)(2,1)S(1)}, bf16[544,128]{1,0:T(8,128)(2,1)S(1)}, u32[]{:S(2)}, u32[]{:S(2)}) collective-permute-start(bf16[544,128]{1,0:T(8,128)(2,1)S(1)} %collective-permute-done.2.rest_1_), channel_id=1, source_target_pairs={{128,256},{192,320},{256,384},{320,448},{129,257},{193,321},{257,3... | collective-permute-start | bytes 417800 | tf_op jit(solution)/shard_map/ppermute | solution.py:536
  85.5 13.2 %collective-permute-start.3 = (bf16[544,128]{1,0:T(8,128)(2,1)S(1)}, bf16[544,128]{1,0:T(8,128)(2,1)S(1)}, u32[]{:S(2)}, u32[]{:S(2)}) collective-permute-start(bf16[544,128]{1,0:T(8,128)(2,1)S(1)} %collective-permute-done.2.rest_1_), channel_id=1, source_target_pairs={{128,192},{192,256},{256,320},{320,384},{384,448},{129,193},{193,2... | collective-permute-start | bytes 417800 | tf_op jit(solution)/shard_map/ppermute | solution.py:536
  98.8 7.4 %copy-start.5 = (f32[2,8,16,64]{3,2,1,0:T(8,128)S(1)}, f32[2,8,16,64]{3,2,1,0:T(8,128)}, u32[]{:S(2)}) copy-start(f32[2,8,16,64]{3,2,1,0:T(8,128)} %param.27) | copy-start | bytes 196612
  98.8 7.5 %copy-start.6 = (f32[8,2,8,64]{3,2,1,0:T(8,128)S(1)}, f32[8,2,8,64]{3,2,1,0:T(8,128)}, u32[]{:S(2)}) copy-start(f32[8,2,8,64]{3,2,1,0:T(8,128)} %init.1) | copy-start | bytes 98308
  102.9 3.3 %copy-start.8 = (f32[8,16]{1,0:T(8,128)S(1)}, f32[8,16]{1,0:T(8,128)}, u32[]{:S(2)}) copy-start(f32[8,16]{1,0:T(8,128)} %skip.1) | copy-start | bytes 1540
  102.9 9.7 %collective-permute-start.8 = (bf16[128,128]{1,0:T(8,128)(2,1)S(1)}, bf16[128,128]{1,0:T(8,128)(2,1)S(1)}, u32[]{:S(2)}, u32[]{:S(2)}) collective-permute-start(bf16[128,128]{1,0:T(8,128)(2,1)S(1)} %get-tuple-element.29), channel_id=1, source_target_pairs={{0,32},{32,0},{1,33},{33,1},{2,34},{34,2},{3,35},{35,3},{4,36},{36... | collective-permute-start | bytes 98312 | tf_op jit(solution)/shard_map/ppermute | solution.py:443
  (2 other events, 1.7 us)

commit v4 on v2

--- a/solution.py
+++ b/solution.py
@@ -415,6 +415,13 @@
     out[...] = dot_nt(acts, weights).astype(bf16)
 
 
+def sum_kernel(shares, out):
+    total = shares[0].astype(f32)
+    for i in range(1, shares.shape[0]):
+        total += shares[i].astype(f32)
+    out[...] = total.astype(bf16)
+
+
 VMEM = pl.BlockSpec(memory_space=pltpu.VMEM)
 SMEM = pl.BlockSpec(memory_space=pltpu.SMEM)
 FAR = pl.BlockSpec(memory_space=pltpu.HBM)
@@ -594,7 +601,8 @@
     )
     parts = partial.reshape(lax.axis_size("tp"), tokens.shape[0], -1)
     shares = lax.all_to_all(parts, "tp", 0, 0, tiled=True)
-    return jnp.sum(shares.astype(f32), axis=0).astype(bf16)
+    (summed,) = call(sum_kernel, [(tokens.shape, bf16)], (), (shares,))
+    return summed
 
 
 def solution(mesh):

time: 126 us -> 126 us (level)
    pallas_call x9 -> x10, Pallas kernels: 13 us -> 13.7 us  [call(): pl.pallas_call(body, out_shape=[jax.ShapeDtypeStruct(s, d) for s, d in ou...]
where the time goes in v4:
time: 126 us; the launch traced here: 125 us
  blocking collectives  47 us (37%)
  waiting for transfers between devices  33.5 us (27%)
  starting transfers between devices  27.2 us (22%)
  Pallas kernels  13.7 us (11%)
  local copies, waits for them, and re-layouts  2.51 us (2%)
    all_to_all x1, blocking collectives, local(): weight_blocks = lax.all_to_all(fanned(weight_rows, Y), Y, 0, 0, tiled=True)  26.3 us
    ppermute x7, starting transfers between devices, along(): return lax.ppermute(x, 'z', pairs)  14.2 us
    pallas_call x10, Pallas kernels, call(): pl.pallas_call(body, out_shape=[jax.ShapeDtypeStruct(s, d) for s, d in ou...  13.7 us
    ppermute x7, waiting for transfers between devices, along(): return lax.ppermute(x, 'z', pairs)  13.7 us
    ppermute x3, waiting for transfers between devices, swapped(): return lax.ppermute(x, axis, [(0, 1), (1, 0)])  13.7 us
    all_to_all x1, blocking collectives, local(): shares = lax.all_to_all(parts, 'tp', 0, 0, tiled=True)  10.5 us
    all_to_all x1, blocking collectives, local(): weight_rows = lax.all_to_all(fan_weights, 'z', 0, 0, tiled=True)  10.2 us
    ppermute x3, starting transfers between devices, swapped(): return lax.ppermute(x, axis, [(0, 1), (1, 0)])  8.55 us
  transfers between devices with their start and end apart: 11, of which 7 were waited for; matrix products, arithmetic and copies ran while one was open for 1% of the time, Pallas kernels for 9%

profile of v4, /device:TPU:392, one launch (start us, length us, event | category | flops | bytes accessed | tf_op | source)
XLA Modules:
  0.0 125.4 jit_solution(18161070333062026302)
XLA Ops:
  0.0 0.9 copy-done.4
  1.8 4.4 %all-to-all-start = ((bf16[4,32,2048]{2,1,0:T(8,128)(2,1)}), bf16[4,32,2048]{2,1,0:T(8,128)(2,1)S(1)}, u32[]{:S(2)}, u32[]{:S(2)}) async-start(bf16[4,32,2048]{2,1,0:T(8,128)(2,1)} %shard_map.164), calls=%async_computation | async-start | bytes 1048576 | tf_op jit(solution)/shard_map/all_to_all | solution.py:479
  9.6 6.1 %all-to-all-done = bf16[4,32,2048]{2,1,0:T(8,128)(2,1)S(1)} async-done(((bf16[4,32,2048]{2,1,0:T(8,128)(2,1)}), bf16[4,32,2048]{2,1,0:T(8,128)(2,1)S(1)}, u32[]{:S(2)}, u32[]{:S(2)}) %all-to-all-start) | async-done | bytes 524320 | tf_op jit(solution)/shard_map/all_to_all | solution.py:479
  15.7 10.2 %all_to_all.20 = bf16[8,16,384]{2,1,0:T(8,128)(2,1)S(1)} all-to-all(bf16[8,16,384]{2,1,0:T(8,128)(2,1)S(1)} %shard_map.163), channel_id=1, replica_groups=mesh['z'=8,'h'=2,'q'=4,'c'=2,'tp'=4] {'z'}, dimensions={0} | all-to-all | bytes 196608 | tf_op jit(solution)/shard_map/all_to_all | solution.py:509
  25.9 26.3 %all_to_all.21 = bf16[8,128,384]{2,1,0:T(8,128)(2,1)S(1)} all-to-all(bf16[8,128,384]{2,1,0:T(8,128)(2,1)S(1)} %shard_map.170), channel_id=1, replica_groups=mesh['z'=8,'h'=2,'q'=4,'c'=2,'tp'=4] {'h','q'}, dimensions={0} | all-to-all | bytes 1572864 | tf_op jit(solution)/shard_map/all_to_all | solution.py:558
  52.3 1.9 %collective-permute-start.9 = (bf16[8,128,384]{2,1,0:T(8,128)(2,1)S(1)}, bf16[8,128,384]{2,1,0:T(8,128)(2,1)S(1)}, u32[]{:S(2)}, u32[]{:S(2)}) collective-permute-start(bf16[8,128,384]{2,1,0:T(8,128)(2,1)S(1)} %all_to_all.21), channel_id=1, source_target_pairs={{0,4},{4,0},{1,5},{5,1},{2,6},{6,2},{3,7},{7,3},{8,12},{12,8},{9,1... | collective-permute-start | bytes 2359304 | tf_op jit(solution)/shard_map/ppermute | solution.py:454
  54.3 3.5 %shard_map.166 = (bf16[400,128]{1,0:T(8,128)(2,1)S(1)}, bf16[400,128]{1,0:T(8,128)(2,1)S(1)}, bf16[128,128]{1,0:T(8,128)(2,1)S(1)}) custom-call(s32[4]{0:T(128)S(1)} %pad_add_fusion.place, bf16[128,2048]{1,0:T(8,128)(2,1)S(1)} %bitcast.19, bf16[2048,256]{1,0:T(8,128)(2,1)S(1)} %copy-done, f32[1,2048]{1,0:T(1,128)} %bitcast.26, bf16[2048,256]{1,0:T(8,128)(2,1)} %w_key_far.1, ...), custom_call_target="tpu_custom_call" | custom-call | tf_op jit(solution)/shard_map/pallas_call | solution.py:433
  57.8 3.4 %collective-permute-start = (bf16[400,128]{1,0:T(8,128)(2,1)S(1)}, bf16[400,128]{1,0:T(8,128)(2,1)S(1)}, u32[]{:S(2)}, u32[]{:S(2)}) collective-permute-start(bf16[400,128]{1,0:T(8,128)(2,1)S(1)} %get-tuple-element.24), channel_id=1, source_target_pairs={{0,32},{32,0},{1,33},{33,1},{2,34},{34,2},{3,35},{35,3},{4,36},{36... | collective-permute-start | bytes 307208 | tf_op jit(solution)/shard_map/ppermute | solution.py:454
  61.1 9.6 %collective-permute-done.got = bf16[400,128]{1,0:T(8,128)(2,1)S(1)} collective-permute-done((bf16[400,128]{1,0:T(8,128)(2,1)S(1)}, bf16[400,128]{1,0:T(8,128)(2,1)S(1)}, u32[]{:S(2)}, u32[]{:S(2)}) %collective-permute-start) | collective-permute-done | bytes 102432 | tf_op jit(solution)/shard_map/ppermute | solution.py:454
  70.7 1.3 %collective-permute-start.5 = (bf16[544,128]{1,0:T(8,128)(2,1)S(1)}, bf16[544,128]{1,0:T(8,128)(2,1)S(1)}, u32[]{:S(2)}, u32[]{:S(2)}) collective-permute-start(bf16[544,128]{1,0:T(8,128)(2,1)S(1)} %shard_map.167), channel_id=1, source_target_pairs={{0,384},{64,448},{128,0},{1,385},{65,449},{129,1},{2,386},{66,450}... | collective-permute-start | bytes 417800 | tf_op jit(solution)/shard_map/ppermute | solution.py:547
  72.0 1.3 %collective-permute-start.2 = (bf16[544,128]{1,0:T(8,128)(2,1)S(1)}, bf16[544,128]{1,0:T(8,128)(2,1)S(1)}, u32[]{:S(2)}, u32[]{:S(2)}) collective-permute-start(bf16[544,128]{1,0:T(8,128)(2,1)S(1)} %shard_map.167), channel_id=1, source_target_pairs={{0,128},{64,192},{128,256},{192,320},{256,384},{320,448},{1,129},{... | collective-permute-start | bytes 417800 | tf_op jit(solution)/shard_map/ppermute | solution.py:547
  74.0 3.6 %collective-permute-start.1 = (bf16[544,128]{1,0:T(8,128)(2,1)S(1)}, bf16[544,128]{1,0:T(8,128)(2,1)S(1)}, u32[]{:S(2)}, u32[]{:S(2)}) collective-permute-start(bf16[544,128]{1,0:T(8,128)(2,1)S(1)} %shard_map.167), channel_id=1, source_target_pairs={{0,64},{64,128},{128,192},{192,256},{256,320},{320,384},{384,448},... | collective-permute-start | bytes 417800 | tf_op jit(solution)/shard_map/ppermute | solution.py:547
  77.6 4.3 %collective-permute-done.5.rest_5_ = bf16[544,128]{1,0:T(8,128)(2,1)S(1)} collective-permute-done((bf16[544,128]{1,0:T(8,128)(2,1)S(1)}, bf16[544,128]{1,0:T(8,128)(2,1)S(1)}, u32[]{:S(2)}, u32[]{:S(2)}) %collective-permute-start.5) | collective-permute-done | bytes 139296 | tf_op jit(solution)/shard_map/ppermute | solution.py:547
  81.9 1.9 %collective-permute-start.6 = (bf16[544,128]{1,0:T(8,128)(2,1)S(1)}, bf16[544,128]{1,0:T(8,128)(2,1)S(1)}, u32[]{:S(2)}, u32[]{:S(2)}) collective-permute-start(bf16[544,128]{1,0:T(8,128)(2,1)S(1)} %collective-permute-done.5.rest_5_), channel_id=1, source_target_pairs={{384,320},{448,384},{0,448},{385,321},{449,385},{1,449},{386,322},... | collective-permute-start | bytes 417800 | tf_op jit(solution)/shard_map/ppermute | solution.py:547
  84.2 1.3 %collective-permute-start.4 = (bf16[544,128]{1,0:T(8,128)(2,1)S(1)}, bf16[544,128]{1,0:T(8,128)(2,1)S(1)}, u32[]{:S(2)}, u32[]{:S(2)}) collective-permute-start(bf16[544,128]{1,0:T(8,128)(2,1)S(1)} %collective-permute-done.2.rest_1_), channel_id=1, source_target_pairs={{128,256},{192,320},{256,384},{320,448},{129,257},{193,321},{257,3... | collective-permute-start | bytes 417800 | tf_op jit(solution)/shard_map/ppermute | solution.py:547
  85.5 4.2 %collective-permute-start.3 = (bf16[544,128]{1,0:T(8,128)(2,1)S(1)}, bf16[544,128]{1,0:T(8,128)(2,1)S(1)}, u32[]{:S(2)}, u32[]{:S(2)}) collective-permute-start(bf16[544,128]{1,0:T(8,128)(2,1)S(1)} %collective-permute-done.2.rest_1_), channel_id=1, source_target_pairs={{128,192},{192,256},{256,320},{320,384},{384,448},{129,193},{193,2... | collective-permute-start | bytes 417800 | tf_op jit(solution)/shard_map/ppermute | solution.py:547
  89.8 4.7 %collective-permute-done.4.rest_3_ = bf16[544,128]{1,0:T(8,128)(2,1)S(1)} collective-permute-done((bf16[544,128]{1,0:T(8,128)(2,1)S(1)}, bf16[544,128]{1,0:T(8,128)(2,1)S(1)}, u32[]{:S(2)}, u32[]{:S(2)}) %collective-permute-start.4) | collective-permute-done | bytes 139296 | tf_op jit(solution)/shard_map/ppermute | solution.py:547
  94.5 4.3 %collective-permute-done.3.rest_2_ = bf16[544,128]{1,0:T(8,128)(2,1)S(1)} collective-permute-done((bf16[544,128]{1,0:T(8,128)(2,1)S(1)}, bf16[544,128]{1,0:T(8,128)(2,1)S(1)}, u32[]{:S(2)}, u32[]{:S(2)}) %collective-permute-start.3) | collective-permute-done | bytes 139296 | tf_op jit(solution)/shard_map/ppermute | solution.py:547
  98.8 4.4 %shard_map.168 = (bf16[128,128]{1,0:T(8,128)(2,1)S(1)}, bf16[128,128]{1,0:T(8,128)(2,1)S(1)}, bf16[224,128]{1,0:T(8,128)(2,1)S(1)}) custom-call(s32[4]{0:T(128)S(1)} %pad_add_fusion.place, f32[2]{0:T(128)S(1)} %copy-done.9, f32[1,128]{1,0:T(1,128)S(1)} %bitcast.25, bf16[400,128]{1,0:T(8,128)(2,1)S(1)} %get-tuple-element.25.keep, ...), custom_call_target="tpu_custom_call" | custom-call | tf_op jit(solution)/shard_map/pallas_call | solution.py:433
  103.2 3.3 %collective-permute-start.8 = (bf16[128,128]{1,0:T(8,128)(2,1)S(1)}, bf16[128,128]{1,0:T(8,128)(2,1)S(1)}, u32[]{:S(2)}, u32[]{:S(2)}) collective-permute-start(bf16[128,128]{1,0:T(8,128)(2,1)S(1)} %get-tuple-element.29), channel_id=1, source_target_pairs={{0,32},{32,0},{1,33},{33,1},{2,34},{34,2},{3,35},{35,3},{4,36},{36... | collective-permute-start | bytes 98312 | tf_op jit(solution)/shard_map/ppermute | solution.py:454
  106.6 2.3 %shard_map.169.state = bf16[128,128]{1,0:T(8,128)(2,1)S(1)} custom-call(s32[4]{0:T(128)S(1)} %pad_add_fusion.place, f32[8,2,8,64]{3,2,1,0:T(8,128)S(1)} %copy-done.6, bf16[400,128]{1,0:T(8,128)(2,1)S(1)} %collective-permute-done.got, bf16[224,128]{1,0:T(8,128)(2,1)S(1)} %get-tuple-element.26.elements, bf16[128,128]{1,0:T(8,128)(2,1)S(1)} %get-tuple-element.27.drive, ...), custom_call_target="tpu_custom_call" | custom-call | tf_op jit(solution)/shard_map/pallas_call | solution.py:433
  108.8 4.1 %collective-permute-done.8.came = bf16[128,128]{1,0:T(8,128)(2,1)S(1)} collective-permute-done((bf16[128,128]{1,0:T(8,128)(2,1)S(1)}, bf16[128,128]{1,0:T(8,128)(2,1)S(1)}, u32[]{:S(2)}, u32[]{:S(2)}) %collective-permute-start.8) | collective-permute-done | bytes 32800 | tf_op jit(solution)/shard_map/ppermute | solution.py:454
  113.0 1.2 shard_map.171
  114.2 10.5 %all_to_all.22.shares = bf16[4,32,2048]{2,1,0:T(8,128)(2,1)S(1)} all-to-all(bf16[4,32,2048]{2,1,0:T(8,128)(2,1)S(1)} %bitcast.18), channel_id=1, replica_groups=mesh['z'=8,'h'=2,'q'=4,'c'=2,'tp'=4] {'tp'}, dimensions={0} | all-to-all | bytes 1048576 | tf_op jit(solution)/shard_map/all_to_all | solution.py:603
  (49 shorter events, 6.2 us)
Async XLA Ops:
  0.0 0.9 copy-start.4
  1.7 4.5 %copy-start.11 = (bf16[256,16]{0,1:T(8,128)(2,1)S(1)}, bf16[256,16]{0,1:T(8,128)(2,1)}, u32[]{:S(2)}) copy-start(bf16[256,16]{0,1:T(8,128)(2,1)} %param.33) | copy-start | bytes 24580
  1.7 4.5 %copy-start.14 = (bf16[128,16]{0,1:T(8,128)(2,1)S(1)}, bf16[128,16]{0,1:T(8,128)(2,1)}, u32[]{:S(2)}) copy-start(bf16[128,16]{0,1:T(8,128)(2,1)} %param.32) | copy-start | bytes 12292
  1.7 4.5 %copy-start.7 = (f32[8,64]{1,0:T(8,128)S(1)}, f32[8,64]{1,0:T(8,128)}, u32[]{:S(2)}) copy-start(f32[8,64]{1,0:T(8,128)} %decay.3) | copy-start | bytes 6148
  1.7 4.5 %copy-start.12 = (f32[8,64]{1,0:T(8,128)S(1)}, f32[8,64]{1,0:T(8,128)}, u32[]{:S(2)}) copy-start(f32[8,64]{1,0:T(8,128)} %param.24) | copy-start | bytes 6148
  1.8 4.6 %copy-start.13 = (f32[128,8]{0,1:T(8,128)S(1)}, f32[128,8]{0,1:T(8,128)}, u32[]{:S(2)}) copy-start(f32[128,8]{0,1:T(8,128)} %param.25) | copy-start | bytes 12292
  1.8 13.9 %all-to-all-start = ((bf16[4,32,2048]{2,1,0:T(8,128)(2,1)}), bf16[4,32,2048]{2,1,0:T(8,128)(2,1)S(1)}, u32[]{:S(2)}, u32[]{:S(2)}) async-start(bf16[4,32,2048]{2,1,0:T(8,128)(2,1)} %shard_map.164), calls=%async_computation | async-start | bytes 1048576 | tf_op jit(solution)/shard_map/all_to_all | solution.py:479
  8.6 17.2 %copy-start.3 = (bf16[2,128,1024]{2,1,0:T(8,128)(2,1)}, bf16[2,128,1024]{2,1,0:T(8,128)(2,1)S(1)}, u32[]{:S(2)}) copy-start(bf16[2,128,1024]{2,1,0:T(8,128)(2,1)S(1)} %get-tuple-element.22.split_far) | copy-start | bytes 1572868
  25.8 28.4 %copy-start = (bf16[2048,256]{1,0:T(8,128)(2,1)S(1)}, bf16[2048,256]{1,0:T(8,128)(2,1)}, u32[]{:S(2)}) copy-start(bf16[2048,256]{1,0:T(8,128)(2,1)} %w_query.1) | copy-start | bytes 3145732
  52.3 60.7 %collective-permute-start.9 = (bf16[8,128,384]{2,1,0:T(8,128)(2,1)S(1)}, bf16[8,128,384]{2,1,0:T(8,128)(2,1)S(1)}, u32[]{:S(2)}, u32[]{:S(2)}) collective-permute-start(bf16[8,128,384]{2,1,0:T(8,128)(2,1)S(1)} %all_to_all.21), channel_id=1, source_target_pairs={{0,4},{4,0},{1,5},{5,1},{2,6},{6,2},{3,7},{7,3},{8,12},{12,8},{9,1... | collective-permute-start | bytes 2359304 | tf_op jit(solution)/shard_map/ppermute | solution.py:454
  57.8 12.9 %collective-permute-start = (bf16[400,128]{1,0:T(8,128)(2,1)S(1)}, bf16[400,128]{1,0:T(8,128)(2,1)S(1)}, u32[]{:S(2)}, u32[]{:S(2)}) collective-permute-start(bf16[400,128]{1,0:T(8,128)(2,1)S(1)} %get-tuple-element.24), channel_id=1, source_target_pairs={{0,32},{32,0},{1,33},{33,1},{2,34},{34,2},{3,35},{35,3},{4,36},{36... | collective-permute-start | bytes 307208 | tf_op jit(solution)/shard_map/ppermute | solution.py:454
  70.7 28.1 %copy-start.9 = (f32[2]{0:T(128)S(1)}, f32[2]{0:T(128)}, u32[]{:S(2)}) copy-start(f32[2]{0:T(128)} %mix.1) | copy-start | bytes 28
  70.7 28.0 %copy-start.10 = (f32[128]{0:T(128)S(1)}, f32[128]{0:T(128)}, u32[]{:S(2)}) copy-start(f32[128]{0:T(128)} %param.31) | copy-start | bytes 1540
  70.7 11.1 %collective-permute-start.5 = (bf16[544,128]{1,0:T(8,128)(2,1)S(1)}, bf16[544,128]{1,0:T(8,128)(2,1)S(1)}, u32[]{:S(2)}, u32[]{:S(2)}) collective-permute-start(bf16[544,128]{1,0:T(8,128)(2,1)S(1)} %shard_map.167), channel_id=1, source_target_pairs={{0,384},{64,448},{128,0},{1,385},{65,449},{129,1},{2,386},{66,450}... | collective-permute-start | bytes 417800 | tf_op jit(solution)/shard_map/ppermute | solution.py:547
  72.0 12.2 %collective-permute-start.2 = (bf16[544,128]{1,0:T(8,128)(2,1)S(1)}, bf16[544,128]{1,0:T(8,128)(2,1)S(1)}, u32[]{:S(2)}, u32[]{:S(2)}) collective-permute-start(bf16[544,128]{1,0:T(8,128)(2,1)S(1)} %shard_map.167), channel_id=1, source_target_pairs={{0,128},{64,192},{128,256},{192,320},{256,384},{320,448},{1,129},{... | collective-permute-start | bytes 417800 | tf_op jit(solution)/shard_map/ppermute | solution.py:547
  73.3 12.2 %collective-permute-start.7 = (bf16[544,128]{1,0:T(8,128)(2,1)S(1)}, bf16[544,128]{1,0:T(8,128)(2,1)S(1)}, u32[]{:S(2)}, u32[]{:S(2)}) collective-permute-start(bf16[544,128]{1,0:T(8,128)(2,1)S(1)} %shard_map.167), channel_id=1, source_target_pairs={{0,448},{1,449},{2,450},{3,451},{4,452},{5,453},{6,454},{7,455},{8... | collective-permute-start | bytes 417800 | tf_op jit(solution)/shard_map/ppermute | solution.py:547
  74.0 15.7 %collective-permute-start.1 = (bf16[544,128]{1,0:T(8,128)(2,1)S(1)}, bf16[544,128]{1,0:T(8,128)(2,1)S(1)}, u32[]{:S(2)}, u32[]{:S(2)}) collective-permute-start(bf16[544,128]{1,0:T(8,128)(2,1)S(1)} %shard_map.167), channel_id=1, source_target_pairs={{0,64},{64,128},{128,192},{192,256},{256,320},{320,384},{384,448},... | collective-permute-start | bytes 417800 | tf_op jit(solution)/shard_map/ppermute | solution.py:547
  81.9 7.9 %collective-permute-start.6 = (bf16[544,128]{1,0:T(8,128)(2,1)S(1)}, bf16[544,128]{1,0:T(8,128)(2,1)S(1)}, u32[]{:S(2)}, u32[]{:S(2)}) collective-permute-start(bf16[544,128]{1,0:T(8,128)(2,1)S(1)} %collective-permute-done.5.rest_5_), channel_id=1, source_target_pairs={{384,320},{448,384},{0,448},{385,321},{449,385},{1,449},{386,322},... | collective-permute-start | bytes 417800 | tf_op jit(solution)/shard_map/ppermute | solution.py:547
  84.2 10.2 %collective-permute-start.4 = (bf16[544,128]{1,0:T(8,128)(2,1)S(1)}, bf16[544,128]{1,0:T(8,128)(2,1)S(1)}, u32[]{:S(2)}, u32[]{:S(2)}) collective-permute-start(bf16[544,128]{1,0:T(8,128)(2,1)S(1)} %collective-permute-done.2.rest_1_), channel_id=1, source_target_pairs={{128,256},{192,320},{256,384},{320,448},{129,257},{193,321},{257,3... | collective-permute-start | bytes 417800 | tf_op jit(solution)/shard_map/ppermute | solution.py:547
  85.5 13.2 %collective-permute-start.3 = (bf16[544,128]{1,0:T(8,128)(2,1)S(1)}, bf16[544,128]{1,0:T(8,128)(2,1)S(1)}, u32[]{:S(2)}, u32[]{:S(2)}) collective-permute-start(bf16[544,128]{1,0:T(8,128)(2,1)S(1)} %collective-permute-done.2.rest_1_), channel_id=1, source_target_pairs={{128,192},{192,256},{256,320},{320,384},{384,448},{129,193},{193,2... | collective-permute-start | bytes 417800 | tf_op jit(solution)/shard_map/ppermute | solution.py:547
  98.8 7.8 %copy-start.5 = (f32[2,8,16,64]{3,2,1,0:T(8,128)S(1)}, f32[2,8,16,64]{3,2,1,0:T(8,128)}, u32[]{:S(2)}) copy-start(f32[2,8,16,64]{3,2,1,0:T(8,128)} %param.27) | copy-start | bytes 196612
  98.8 7.8 %copy-start.6 = (f32[8,2,8,64]{3,2,1,0:T(8,128)S(1)}, f32[8,2,8,64]{3,2,1,0:T(8,128)}, u32[]{:S(2)}) copy-start(f32[8,2,8,64]{3,2,1,0:T(8,128)} %init.1) | copy-start | bytes 98308
  103.2 3.3 %copy-start.8 = (f32[8,16]{1,0:T(8,128)S(1)}, f32[8,16]{1,0:T(8,128)}, u32[]{:S(2)}) copy-start(f32[8,16]{1,0:T(8,128)} %skip.1) | copy-start | bytes 1540
  103.2 9.7 %collective-permute-start.8 = (bf16[128,128]{1,0:T(8,128)(2,1)S(1)}, bf16[128,128]{1,0:T(8,128)(2,1)S(1)}, u32[]{:S(2)}, u32[]{:S(2)}) collective-permute-start(bf16[128,128]{1,0:T(8,128)(2,1)S(1)} %get-tuple-element.29), channel_id=1, source_target_pairs={{0,32},{32,0},{1,33},{33,1},{2,34},{34,2},{3,35},{35,3},{4,36},{36... | collective-permute-start | bytes 98312 | tf_op jit(solution)/shard_map/ppermute | solution.py:454
  (2 other events, 1.7 us)
